TPU v7x, 256 devices: a whole 4x4x8 slice. The times are simulated.
256 devices in a mesh: sp: 32 (over z, y), tp: 8 (over x, core).
Axes of the slice: x: 4, y: 4, z: 8, core: 2. Of those that a mesh axis runs over, the one named last changes fastest.
Arguments:
- skip_stream: bfloat16 [24576, 2048], P(('sp', 'tp')), may hold values from -24 to 24
- acceptance_signal: bfloat16 [24576, 2048], P('sp', 'tp'), may hold values from -6 to 6
- lookup_mapped: bfloat16 [24576, 2048], P('sp', 'tp'), may hold values from -12 to 12
- payload_mapped: bfloat16 [24576, 2048], P('sp', 'tp'), may hold values from -6 to 6
- result_switch: bfloat16 [24576, 2048], P('sp', 'tp'), may hold values from -6 to 6
- forget_dynamic_share: bfloat16 [24576, 2048], P('sp', 'tp'), may hold values from -4 to 4
- additive_forget_logarithm: float32 [24576, 32], P('sp', 'tp'), may hold values from -1 to 0
- forget_feature_offset: float32 [2048], P('tp'), may hold values from -11 to -3
- substitution_dynamic_share: bfloat16 [24576, 2048], P('sp', 'tp'), may hold values from -6 to 6
- substitution_feature_offset: float32 [2048], P('tp'), may hold values from -6.5 to 2.5
- diagonal_reward_scales: float32 [2048], P('tp'), may hold values from -0.9 to 0.9
- result_matrix: bfloat16 [2048, 2048], P('tp'), may hold values from -0.125 to 0.125
- mlp_rescaler: float32 [2048], replicated, may hold values from 0.1 to 1.9
- switch_matrix: bfloat16 [2048, 5120], P('sp', 'tp'), may hold values from -0.125 to 0.125
- expand_matrix: bfloat16 [2048, 5120], P('sp', 'tp'), may hold values from -0.125 to 0.125
- contract_matrix: bfloat16 [2048, 5120], P('sp', 'tp'), may hold values from -0.25 to 0.25
Outputs:
- mixed_out: bfloat16 [24576, 2048], P(('sp', 'tp'))
All inputs are finite; a program needn't handle non-finite values.
Results may differ from a plain program's by a relative error of at most 0.015.
Values may be sent and summed in bfloat16 or wider, within the bound.
A program may use at most 128 MiB of HBM per device.

v0:
```python
import jax
import jax.numpy as jnp
from jax import lax
from jax.sharding import Mesh
from jax.sharding import PartitionSpec as P

PER_GROUP_DIMS = 64
SP = ("sp_0", "sp_1")
SP_TP = ("sp_0", "sp_1", "tp")


norm_eps = 1e-06
group_eps = 0.00064
half_step = 0.5


def side_by_side(arrays, axis, dim, along):
    widths = [a.shape[along] for a in arrays]
    both = jnp.concatenate(arrays, axis=along)
    result = lax.all_gather(both, axis, axis=dim, tiled=True)
    return tuple(jnp.split(result, [sum(widths[:k]) for k in range(1, len(widths))], axis=along))


def filled_with(shard, identity):
    return jax.tree.map(
        lambda a, e: jnp.broadcast_to(jnp.asarray(e, a.dtype), a.shape), shard, identity
    )


def carried_in(shard, axes, combine, identity):
    before = start = filled_with(shard, identity)
    so_far = shard
    for axis in reversed(axes):
        peers, place = (lax.axis_size(axis), lax.axis_index(axis))
        pieces = jax.tree.map(
            lambda part, kind: lax.all_gather(part.astype(kind), axis),
            so_far,
            (jnp.bfloat16, jnp.bfloat16),
        )
        inside, so_far = (start, start)
        for k in range(peers):
            passed = k < place
            so_far = combine(
                so_far, jax.tree.map(lambda part, own: part[k].astype(own.dtype), pieces, shard)
            )
            inside = jax.tree.map(lambda new, old: jnp.where(passed, new, old), so_far, inside)
        before = combine(inside, before)
    return before


def split_up(shard, dim, peers):
    before, after = (shard.shape[:dim], shard.shape[dim + 1 :])
    return jnp.moveaxis(shard.reshape(*before, peers, -1, *after), dim, 0)


def sent_and_summed(shard, axis, dim):
    peers = lax.axis_size(axis)
    parts = lax.all_to_all(split_up(shard, dim, peers), axis, 0, 0, tiled=True)
    return jnp.sum(parts.astype(jnp.float32), axis=0)


def compose(earlier, latter):
    prod_first, carry_first = earlier
    prod_second, carry_second = latter
    product = jnp.einsum("hij,hjk->hik", prod_first, prod_second)
    carried = jnp.einsum("hij,hjk->hik", carry_first, prod_second) + carry_second
    return (product, carried)


def masked_pairs(left, right, keep):
    return jnp.where(keep, jnp.einsum("htc,hjc->htj", left, right), 0.0)


def block_step(carry, inputs):
    state_part, transition = carry
    read_blk, logstep_blk, key_blk, value_blk, unit_blk, rate_blk = inputs
    length = read_blk.shape[1]
    width = value_blk.shape[2]
    cumulate = jnp.cumsum(logstep_blk, axis=1)
    growth = jnp.exp(cumulate)
    shrink = jnp.exp(-cumulate)
    before_unit = jnp.exp(cumulate - logstep_blk) * unit_blk
    erase_dir = unit_blk * rate_blk
    key_back = key_blk * shrink
    erase_back = erase_dir * shrink
    read_fwd = read_blk * growth
    end_growth = growth[:, -1:, :]
    key_end = key_back * end_growth
    erase_end = erase_back * end_growth
    row_index = lax.broadcasted_iota(jnp.int32, (length, length), 0)
    col_index = lax.broadcasted_iota(jnp.int32, (length, length), 1)
    strict = col_index < row_index
    inclusive = col_index <= row_index
    key_past = masked_pairs(before_unit, key_back, strict)
    erase_past = masked_pairs(before_unit, erase_back, strict)
    key_read = masked_pairs(read_fwd, key_back, inclusive)
    erase_read = masked_pairs(read_fwd, erase_back, inclusive)
    recall_rhs = jnp.einsum("htk,hvk->htv", before_unit, state_part) + jnp.einsum(
        "htj,hjv->htv", key_past, value_blk
    )
    solved = jax.scipy.linalg.solve_triangular(
        erase_past,
        jnp.concatenate([recall_rhs, before_unit], axis=-1),
        lower=True,
        unit_diagonal=True,
    )
    recalled = solved[..., :width]
    carried_map = solved[..., width:]
    local_out = (
        jnp.einsum("htk,hvk->htv", read_fwd, state_part)
        + jnp.einsum("htj,hjv->htv", key_read, value_blk)
        - jnp.einsum("htj,hjv->htv", erase_read, recalled)
    )
    from_start = read_fwd - jnp.einsum("htj,hjk->htk", erase_read, carried_map)
    coefficient = jnp.einsum("htk,hjk->htj", from_start, transition)
    new_state = (
        state_part * end_growth
        + jnp.einsum("htv,htk->hvk", value_blk, key_end)
        - jnp.einsum("htv,htk->hvk", recalled, erase_end)
    )
    step_map = jnp.eye(width, dtype=jnp.float32)[None] * end_growth - jnp.einsum(
        "htj,htk->hjk", carried_map, erase_end
    )
    new_transition = jnp.einsum("hij,hjk->hik", transition, step_map)
    return ((new_state, new_transition), (local_out, coefficient))


def per_device(
    skip_stream,
    acceptance_signal,
    lookup_mapped,
    payload_mapped,
    result_switch,
    forget_dynamic_share,
    additive_forget_logarithm,
    forget_feature_offset,
    substitution_dynamic_share,
    substitution_feature_offset,
    diagonal_reward_scales,
    result_matrix,
    mlp_rescaler,
    switch_matrix,
    expand_matrix,
    contract_matrix,
):
    matrix_length, matrix_breadth = acceptance_signal.shape
    attention_groups = matrix_breadth // PER_GROUP_DIMS
    gate_whole, up_whole, down_whole = side_by_side(
        (switch_matrix, expand_matrix, contract_matrix), SP, 0, 1
    )

    def by_head(values):
        return values.astype(jnp.float32).reshape(matrix_length, attention_groups, PER_GROUP_DIMS)

    acceptance_lines = by_head(acceptance_signal)
    lookup_vectors = by_head(lookup_mapped)
    payload_vectors = by_head(payload_mapped)
    log_decay_rate = (
        -jax.nn.softplus(
            -(forget_feature_offset[None, :] + forget_dynamic_share.astype(jnp.float32))
        )
        - 0.5
    )
    log_step = (
        -jnp.exp(log_decay_rate).reshape(matrix_length, attention_groups, PER_GROUP_DIMS)
        + additive_forget_logarithm[:, :, None]
    )
    replace_rate = jax.nn.sigmoid(
        substitution_feature_offset[None, :] + substitution_dynamic_share.astype(jnp.float32)
    )
    replace_rate = replace_rate.reshape(matrix_length, attention_groups, PER_GROUP_DIMS)
    unit_key = lookup_vectors * lax.rsqrt(
        jnp.sum(lookup_vectors * lookup_vectors, axis=-1, keepdims=True) + norm_eps
    )
    block_len = min(64, matrix_length)
    block_count = matrix_length // block_len

    def to_blocks(values):
        return values.reshape(block_count, block_len, attention_groups, PER_GROUP_DIMS).transpose(
            0, 2, 1, 3
        )

    def from_blocks(values):
        return values.transpose(0, 2, 1, 3).reshape(matrix_length, attention_groups, PER_GROUP_DIMS)

    identity_mats = jnp.broadcast_to(
        jnp.eye(PER_GROUP_DIMS, dtype=jnp.float32),
        (attention_groups, PER_GROUP_DIMS, PER_GROUP_DIMS),
    )
    zero_mats = jnp.zeros((attention_groups, PER_GROUP_DIMS, PER_GROUP_DIMS), jnp.float32)
    (closing_state, closing_map), (local_blocks, coef_blocks) = lax.scan(
        block_step,
        (zero_mats, identity_mats),
        (
            to_blocks(acceptance_lines),
            to_blocks(log_step),
            to_blocks(lookup_vectors),
            to_blocks(payload_vectors),
            to_blocks(unit_key),
            to_blocks(replace_rate),
        ),
    )
    _, carried = carried_in((closing_map, closing_state), SP, compose, (identity_mats, zero_mats))
    outcome = from_blocks(local_blocks) + jnp.einsum(
        "hvk,thk->thv", carried, from_blocks(coef_blocks)
    )
    centre = jnp.mean(outcome, axis=-1, keepdims=True)
    spread = jnp.mean(jnp.square(outcome - centre), axis=-1, keepdims=True)
    rescaled_attention = (outcome - centre) * lax.rsqrt(spread + group_eps)
    diagonal_reward_summand = (
        jnp.sum(
            acceptance_lines
            * lookup_vectors
            * diagonal_reward_scales.reshape(attention_groups, PER_GROUP_DIMS),
            axis=-1,
            keepdims=True,
        )
        * payload_vectors
    )
    merged_attention = (
        (rescaled_attention + diagonal_reward_summand).reshape(matrix_length, matrix_breadth)
        * result_switch.astype(jnp.float32)
    ).astype(jnp.bfloat16)
    row_block = merged_attention
    projected = sent_and_summed(
        jnp.dot(row_block, result_matrix, preferred_element_type=jnp.float32).astype(jnp.bfloat16),
        "tp",
        0,
    ).astype(jnp.bfloat16)
    stream = skip_stream.astype(jnp.float32) + lax.optimization_barrier(projected).astype(
        jnp.float32
    )
    scale_rows = lax.rsqrt(jnp.mean(stream * stream, axis=-1, keepdims=True) + norm_eps)
    normed_rows = (stream * scale_rows * mlp_rescaler[None, :]).astype(jnp.bfloat16)
    whole_rows = lax.all_gather(normed_rows, "tp", axis=0, tiled=True)
    gate_act = jnp.dot(whole_rows, gate_whole, preferred_element_type=jnp.float32)
    up_act = jnp.dot(whole_rows, up_whole, preferred_element_type=jnp.float32)
    hidden = (jax.nn.silu(gate_act) * up_act).astype(jnp.bfloat16)
    row_block = hidden
    ffn_out = lax.psum_scatter(
        lax.dot_general(
            row_block, down_whole, (((1,), (1,)), ((), ())), preferred_element_type=jnp.float32
        ).astype(jnp.bfloat16),
        "tp",
        scatter_dimension=0,
        tiled=True,
    )
    return (stream + half_step * lax.optimization_barrier(ffn_out).astype(jnp.float32)).astype(
        jnp.bfloat16
    )


def solution(mesh):
    torus = Mesh(mesh.devices.reshape(8, 4, mesh.shape["tp"]), ("sp_0", "sp_1", "tp"))
    in_specs = (
        P(SP_TP, None),
        P(SP, "tp"),
        P(SP, "tp"),
        P(SP, "tp"),
        P(SP, "tp"),
        P(SP, "tp"),
        P(SP, "tp"),
        P("tp"),
        P(SP, "tp"),
        P("tp"),
        P("tp"),
        P("tp", None),
        P(),
        P(SP, "tp"),
        P(SP, "tp"),
        P(SP, "tp"),
    )
    out_specs = P(SP_TP, None)
    return jax.shard_map(
        per_device, mesh=torus, in_specs=in_specs, out_specs=out_specs, check_vma=False
    )
```

profile of v0, /device:TPU:1, one launch (start us, length us, event | category | flops | bytes accessed | tf_op | source)
XLA Modules:
  0.0 706.1 jit_solution(7916593708579089121)
XLA Ops:
  28.2 4.9 multiply_bitcast_fusion
  33.1 339.6 %while.17 = (s32[]{:T(128)}, f32[4,64,64]{2,1,0:T(8,128)S(1)}, bf16[4,64,64]{1,2,0:T(8,128)(2,1)S(1)}, f32[12,4,64,64]{3,2,1,0:T(8,128)}, bf16[12,4,64,64]{3,2,1...) while((s32[]{:T(128)}, f32[4,64,64]{2,1,0:T(8,128)S(1)}, ...), condition=%wide.region_3.4_spmd.clone, body=%wide.region_1.3_spmd.clone.sunk | while | flops 58290240 | bytes 4974245 | solution.py:191
  38.1 19.7 %custom-call.9 = f32[4,1,64,64]{2,3,1,0:T(8,128)S(1)} custom-call(f32[4,1,64,64]{3,2,1,0:T(8,128)S(1)} %fusion.259), custom_call_target="InvertDiagBlocksLowerTriangular" | custom-call | tf_op jit(solution)/shard_map/while/body/eval_jaxpr/jit(_solve_triangular)/vmap()/triangular_solve | solution.py:101
  66.5 19.7 %custom-call.9 = f32[4,1,64,64]{2,3,1,0:T(8,128)S(1)} custom-call(f32[4,1,64,64]{3,2,1,0:T(8,128)S(1)} %fusion.259), custom_call_target="InvertDiagBlocksLowerTriangular" | custom-call | tf_op jit(solution)/shard_map/while/body/eval_jaxpr/jit(_solve_triangular)/vmap()/triangular_solve | solution.py:101
  94.7 19.7 %custom-call.9 = f32[4,1,64,64]{2,3,1,0:T(8,128)S(1)} custom-call(f32[4,1,64,64]{3,2,1,0:T(8,128)S(1)} %fusion.259), custom_call_target="InvertDiagBlocksLowerTriangular" | custom-call | tf_op jit(solution)/shard_map/while/body/eval_jaxpr/jit(_solve_triangular)/vmap()/triangular_solve | solution.py:101
  123.0 19.7 %custom-call.9 = f32[4,1,64,64]{2,3,1,0:T(8,128)S(1)} custom-call(f32[4,1,64,64]{3,2,1,0:T(8,128)S(1)} %fusion.259), custom_call_target="InvertDiagBlocksLowerTriangular" | custom-call | tf_op jit(solution)/shard_map/while/body/eval_jaxpr/jit(_solve_triangular)/vmap()/triangular_solve | solution.py:101
  151.3 19.7 %custom-call.9 = f32[4,1,64,64]{2,3,1,0:T(8,128)S(1)} custom-call(f32[4,1,64,64]{3,2,1,0:T(8,128)S(1)} %fusion.259), custom_call_target="InvertDiagBlocksLowerTriangular" | custom-call | tf_op jit(solution)/shard_map/while/body/eval_jaxpr/jit(_solve_triangular)/vmap()/triangular_solve | solution.py:101
  179.6 19.7 %custom-call.9 = f32[4,1,64,64]{2,3,1,0:T(8,128)S(1)} custom-call(f32[4,1,64,64]{3,2,1,0:T(8,128)S(1)} %fusion.259), custom_call_target="InvertDiagBlocksLowerTriangular" | custom-call | tf_op jit(solution)/shard_map/while/body/eval_jaxpr/jit(_solve_triangular)/vmap()/triangular_solve | solution.py:101
  207.9 19.7 %custom-call.9 = f32[4,1,64,64]{2,3,1,0:T(8,128)S(1)} custom-call(f32[4,1,64,64]{3,2,1,0:T(8,128)S(1)} %fusion.259), custom_call_target="InvertDiagBlocksLowerTriangular" | custom-call | tf_op jit(solution)/shard_map/while/body/eval_jaxpr/jit(_solve_triangular)/vmap()/triangular_solve | solution.py:101
  236.2 19.7 %custom-call.9 = f32[4,1,64,64]{2,3,1,0:T(8,128)S(1)} custom-call(f32[4,1,64,64]{3,2,1,0:T(8,128)S(1)} %fusion.259), custom_call_target="InvertDiagBlocksLowerTriangular" | custom-call | tf_op jit(solution)/shard_map/while/body/eval_jaxpr/jit(_solve_triangular)/vmap()/triangular_solve | solution.py:101
  264.5 19.7 %custom-call.9 = f32[4,1,64,64]{2,3,1,0:T(8,128)S(1)} custom-call(f32[4,1,64,64]{3,2,1,0:T(8,128)S(1)} %fusion.259), custom_call_target="InvertDiagBlocksLowerTriangular" | custom-call | tf_op jit(solution)/shard_map/while/body/eval_jaxpr/jit(_solve_triangular)/vmap()/triangular_solve | solution.py:101
  292.8 19.7 %custom-call.9 = f32[4,1,64,64]{2,3,1,0:T(8,128)S(1)} custom-call(f32[4,1,64,64]{3,2,1,0:T(8,128)S(1)} %fusion.259), custom_call_target="InvertDiagBlocksLowerTriangular" | custom-call | tf_op jit(solution)/shard_map/while/body/eval_jaxpr/jit(_solve_triangular)/vmap()/triangular_solve | solution.py:101
  321.1 19.7 %custom-call.9 = f32[4,1,64,64]{2,3,1,0:T(8,128)S(1)} custom-call(f32[4,1,64,64]{3,2,1,0:T(8,128)S(1)} %fusion.259), custom_call_target="InvertDiagBlocksLowerTriangular" | custom-call | tf_op jit(solution)/shard_map/while/body/eval_jaxpr/jit(_solve_triangular)/vmap()/triangular_solve | solution.py:101
  349.4 19.7 %custom-call.9 = f32[4,1,64,64]{2,3,1,0:T(8,128)S(1)} custom-call(f32[4,1,64,64]{3,2,1,0:T(8,128)S(1)} %fusion.259), custom_call_target="InvertDiagBlocksLowerTriangular" | custom-call | tf_op jit(solution)/shard_map/while/body/eval_jaxpr/jit(_solve_triangular)/vmap()/triangular_solve | solution.py:101
  372.8 11.2 %all-gather = bf16[16,64,64]{2,1,0:T(8,128)(2,1)S(1)} all-gather(bf16[4,64,64]{2,1,0:T(8,128)(2,1)S(1)} %copy.76), channel_id=2, replica_groups=mesh['sp_0'=8,'sp_1'=4,'tp'=8] {'sp_1'}, dimensions={0}, use_global_device_ids=true | all-gather | bytes 163840 | tf_op jit(solution)/shard_map/all_gather | solution.py:36
  384.0 9.8 %all-gather.2 = bf16[16,64,64]{2,1,0:T(8,128)(2,1)S(1)} all-gather(bf16[4,64,64]{2,1,0:T(8,128)(2,1)S(1)} %convert_element_type.170), channel_id=4, replica_groups=mesh['sp_0'=8,'sp_1'=4,'tp'=8] {'sp_1'}, dimensions={0}, use_global_device_ids=true | all-gather | bytes 163840 | tf_op jit(solution)/shard_map/all_gather | solution.py:36
  396.2 23.0 %all-gather.3 = bf16[32,64,64]{2,1,0:T(8,128)(2,1)S(1)} all-gather(bf16[4,64,64]{2,1,0:T(8,128)(2,1)S(1)} %convolution_add_fusion.10), channel_id=5, replica_groups=mesh['sp_0'=8,'sp_1'=4,'tp'=8] {'sp_0'}, dimensions={0}, use_global_device_ids=true | all-gather | bytes 294912 | tf_op jit(solution)/shard_map/all_gather | solution.py:36
  420.3 19.5 %all-gather.1 = bf16[32,64,64]{2,1,0:T(8,128)(2,1)S(1)} all-gather(bf16[4,64,64]{2,1,0:T(8,128)(2,1)S(1)} %fusion.143), channel_id=3, replica_groups=mesh['sp_0'=8,'sp_1'=4,'tp'=8] {'sp_0'}, dimensions={0}, use_global_device_ids=true | all-gather | bytes 294912 | tf_op jit(solution)/shard_map/all_gather | solution.py:36
  457.9 59.3 %all_to_all.5 = bf16[8,96,2048]{2,1,0:T(8,128)(2,1)} all-to-all(bf16[8,96,2048]{2,1,0:T(8,128)(2,1)S(1)} %bitcast.166), channel_id=1, replica_groups=mesh['sp_0'=8,'sp_1'=4,'tp'=8] {'tp'}, dimensions={0} | all-to-all | bytes 6291456 | tf_op jit(solution)/shard_map/all_to_all | solution.py:58
  522.1 26.9 %all-gather.7.cloned.1.call-done = bf16[768,2048]{1,0:T(8,128)(2,1)} async-done(((bf16[96,2048]{1,0:T(8,128)(2,1)}), bf16[768,2048]{1,0:T(8,128)(2,1)}) %all-gather.7.cloned.1.call-update) | async-done | bytes 3145744 | tf_op jit(solution)/shard_map/all_gather | solution.py:235
  549.0 96.7 %all-gather.9.cloned.1.call-done = bf16[2048,1920]{1,0:T(8,128)(2,1)} async-done(((bf16[64,1920]{1,0:T(8,128)(2,1)}), bf16[2048,1920]{1,0:T(8,128)(2,1)}) %all-gather.9.cloned.1.call-update) | async-done | bytes 7864336 | tf_op jit(solution)/shard_map/all_gather | solution.py:20
  645.6 6.6 fusion.62
  652.2 11.6 %convolution_convert_fusion = bf16[768,2048]{1,0:T(8,128)(2,1)} fusion(bf16[2048,1920]{1,0:T(8,128)(2,1)} %all-gather.9.cloned.1.call-done, f32[768,640]{1,0:T(8,128)} %fusion.62, bf16[768,2048]{1,0:T(8,128)(2,1)} %all-gather.7.cloned.1.call-done), kind=kOutput, calls=%fused_computation.82 | convolution fusion | flops 4031053824 | bytes 13500416 | tf_op jit(solution)/shard_map/dot_general | solution.py:241
  663.8 33.9 %reduce-scatter.2.cloned.1.call-done = bf16[96,2048]{1,0:T(8,128)(2,1)} async-done(((bf16[768,2048]{1,0:T(8,128)(2,1)}), bf16[96,2048]{1,0:T(8,128)(2,1)}) %reduce-scatter.2.cloned.1.call-update) | async-done | bytes 393232 | tf_op jit(solution)/shard_map/reduce_scatter | solution.py:240
  (452 shorter events, 151.6 us)
Async XLA Ops:
  6.5 450.4 %copy-start = (bf16[256,2048]{1,0:T(8,128)(2,1)S(1)}, bf16[256,2048]{1,0:T(8,128)(2,1)}, u32[]{:S(2)}) copy-start(bf16[256,2048]{1,0:T(8,128)(2,1)} %param.29) | copy-start | bytes 3145732
  6.5 2.2 copy-start.7
  6.5 542.4 %all-gather.7.cloned.1.call-start = ((), (), s32[]{:S(2)}) async-start(), calls=%async_computation.2 | async-start | bytes 3538944 | tf_op jit(solution)/shard_map/all_gather | solution.py:235
  12.6 3.9 copy-start.27
  12.6 4.9 copy-start.8
  12.6 4.9 copy-start.30
  28.1 4.9 copy-start.23
  393.9 25.6 %copy-start.10 = (bf16[4,64,64]{2,1,0:T(8,128)(2,1)}, bf16[4,64,64]{2,1,0:T(8,128)(2,1)S(1)}, u32[]{:S(2)}) copy-start(bf16[4,64,64]{2,1,0:T(8,128)(2,1)S(1)} %fusion.116) | copy-start | bytes 98308
  419.2 22.8 %copy-start.4 = (bf16[32,64,64]{2,1,0:T(8,128)(2,1)}, bf16[32,64,64]{2,1,0:T(8,128)(2,1)S(1)}, u32[]{:S(2)}) copy-start(bf16[32,64,64]{2,1,0:T(8,128)(2,1)S(1)} %all-gather.3) | copy-start | bytes 786436
  439.8 2.2 copy-start.5
  440.8 4.8 copy-start.11
  441.0 4.7 copy-start.12
  441.1 4.5 copy-start.13
  447.0 3.3 copy-start.17
  447.0 3.3 copy-start.19
  447.0 3.3 copy-start.26
  450.5 3.8 copy-start.2
  450.5 3.8 copy-start.3
  452.5 1.7 copy-start.29
  455.5 1.5 copy-start.6
  517.2 2.5 copy-start.1
  517.2 2.8 copy-start.28
  521.0 124.7 %all-gather.9.cloned.1.call-start = ((), (), s32[]{:S(2)}) async-start(), calls=%async_computation.3 | async-start | bytes 8110080 | tf_op jit(solution)/shard_map/all_gather | solution.py:20
  521.8 175.9 %reduce-scatter.2.cloned.1.call-start = ((), (), s32[]{:S(2)}) async-start(), calls=%async_computation.4 | async-start | bytes 3538944 | tf_op jit(solution)/shard_map/reduce_scatter | solution.py:240
  (10 other events, 8.2 us)
Sparse Core Ops, SparseCore 0:
  521.1 27.8 all-gather.6
  551.5 94.0 all-gather.8
  664.0 33.6 reduce-scatter.1
where the time goes:
time: 710 us; the launch traced here: 706 us
  other arithmetic  257 us (36%)
  waiting for transfers between devices  157 us (22%)
  blocking collectives  123 us (17%)
  local copies, waits for them, and re-layouts  76.8 us (11%)
  matrix products  76.8 us (11%)
  between operations  13.5 us (2%)
    another operation x36, other arithmetic, block_step(): jax.scipy.linalg.solve_triangular(erase_past, jnp.concatenate([recall_rhs...  236 us
    all_gather x1, waiting for transfers between devices, side_by_side(): result = lax.all_gather(both, axis, axis=dim, tiled=True)  96.7 us
    all_gather x4, blocking collectives, carried_in(): lax.all_gather(part.astype(kind), axis)  63.5 us
    all_to_all x1, blocking collectives, sent_and_summed(): parts = lax.all_to_all(split_up(shard, dim, peers), axis, 0, 0, tiled=True)  59.3 us
    dynamic_slice x72, local copies, waits for them, and re-layouts, per_device(): lax.scan(block_step, (zero_mats, identity_mats), (to_blocks(acceptance_li...  46.8 us
    reduce_scatter x1, waiting for transfers between devices, per_device(): lax.psum_scatter(lax.dot_general(row_block, down_whole, (((1,), (1,)), ((...  33.9 us
    all_gather x1, waiting for transfers between devices, per_device(): whole_rows = lax.all_gather(normed_rows, 'tp', axis=0, tiled=True)  26.9 us
  transfers between devices with their start and end apart: 3, of which 3 were waited for; matrix products, arithmetic and copies ran while one was open for 0% of the time, Pallas kernels for 0%

commit v1 on v0

v1 whole, which is shorter than its diff:
```python
import functools

import jax
import jax.numpy as jnp
from jax import lax
from jax.experimental import pallas as pl
from jax.experimental.pallas import tpu as pltpu
from jax.sharding import Mesh
from jax.sharding import PartitionSpec as P

PER_GROUP_DIMS = 64
SP = ("sp_0", "sp_1")
SP_TP = ("sp_0", "sp_1", "tp")
MESH = pl.DeviceIdType.MESH

norm_eps = 1e-06
group_eps = 0.00064
half_step = 0.5
EXP_HALF = 0.6065306597126334

C = 64
TOGETHER = 2
LEVELS = (2, 4, 8, 16, 32)
F32 = jnp.float32
BF16 = jnp.bfloat16


def dot_nn(a, b):
    return lax.dot_general(a, b, (((1,), (0,)), ((), ())), preferred_element_type=F32)


def dot_nt(a, b):
    return lax.dot_general(a, b, (((1,), (1,)), ((), ())), preferred_element_type=F32)


def dot_tn(a, b):
    return lax.dot_general(a, b, (((0,), (0,)), ((), ())), preferred_element_type=F32)


def two_parts(x):
    high = x.astype(BF16)
    return high, (x - high.astype(F32)).astype(BF16)


def mixing_kernel(
    n_z,
    n_y,
    r_ref,
    k_ref,
    v_ref,
    gate_ref,
    fd_ref,
    afl_ref,
    foff_ref,
    sd_ref,
    soff_ref,
    scale_ref,
    out_ref,
    mask_ref,
    level_ref,
    local_ref,
    coef_ref,
    extra_ref,
    sm_ref,
    packet_y,
    recv_y,
    packet_z,
    recv_z,
    s_ref,
    send_y_sem,
    recv_y_sem,
    send_z_sem,
    recv_z_sem,
):
    length, width = r_ref.shape
    heads = width // C
    place_z = lax.axis_index("sp_0")
    place_y = lax.axis_index("sp_1")

    barrier = pltpu.get_barrier_semaphore()
    for d in range(1, n_y):
        pl.semaphore_signal(
            barrier, inc=1, device_id={"sp_1": lax.rem(place_y + d, n_y)}, device_id_type=MESH
        )
    for d in range(1, n_z):
        pl.semaphore_signal(
            barrier, inc=1, device_id={"sp_0": lax.rem(place_z + d, n_z)}, device_id_type=MESH
        )

    big_row = lax.broadcasted_iota(jnp.int32, (width, width), 0)
    big_col = lax.broadcasted_iota(jnp.int32, (width, width), 1)
    same_head = (big_row // C) == (big_col // C)
    mask_ref[...] = jnp.where(same_head, 1.0, 0.0).astype(BF16)

    t_idx = lax.broadcasted_iota(jnp.int32, (C, width), 0)
    lane = lax.broadcasted_iota(jnp.int32, (C, width), 1)
    j_idx = lane % C
    strict = j_idx < t_idx
    inclusive = j_idx <= t_idx
    eye = jnp.where(j_idx == t_idx, 1.0, 0.0).astype(F32)
    for n, b in enumerate(LEVELS):
        rb = (big_row % C) // b
        cb = (big_col % C) // b
        level_ref[n] = jnp.where(
            same_head & (rb % 2 == 1) & (cb == rb - 1), 1.0, 0.0
        ).astype(BF16)
    first_level = (t_idx % 2 == 1) & (j_idx == t_idx - 1)

    tri = jnp.where(
        (lax.broadcasted_iota(jnp.int32, (C, 2 * C), 1) % C)
        <= lax.broadcasted_iota(jnp.int32, (C, 2 * C), 0),
        1.0,
        0.0,
    ).astype(BF16)

    def tiled(x):
        return jnp.concatenate([x.astype(BF16)] * heads, axis=0)

    def bd(x):
        return tiled(x) * mask_ref[...]

    def diagonal_of(full):
        out = full[0:C]
        for h in range(1, heads):
            out = jnp.where(lane >= h * C, full[h * C : (h + 1) * C], out)
        return out

    sm_ref[0:C, :] = jnp.zeros((C, width), F32)
    sm_ref[C:, :] = eye

    def chunk(c, result):
        rows = pl.ds(pl.multiple_of(c * C, C), C)
        r = r_ref[rows, :].astype(F32)
        k = k_ref[rows, :].astype(F32)
        vb = v_ref[rows, :]
        v = vb.astype(F32)
        afl = afl_ref[rows, :]
        added = jnp.broadcast_to(afl[:, 0:1], (C, width))
        for h in range(1, heads):
            added = jnp.where(lane >= h * C, afl[:, h : h + 1], added)
        log_step = added - EXP_HALF * jax.nn.sigmoid(foff_ref[...] + fd_ref[rows, :].astype(F32))
        rate = jax.nn.sigmoid(soff_ref[...] + sd_ref[rows, :].astype(F32))
        k_hi, k_lo = two_parts(k * k)
        d_hi, d_lo = two_parts(r * k * scale_ref[...])
        sums = dot_nn(jnp.concatenate([k_hi, k_lo, d_hi, d_lo], axis=0), mask_ref[...])
        l_hi, l_lo = two_parts(log_step)
        cum = dot_nn(tri, jnp.concatenate([l_hi, l_lo], axis=0))
        yield
        unit = k * lax.rsqrt(sums[0:C] + sums[C : 2 * C] + norm_eps)
        extra_ref[rows, :] = (sums[2 * C : 3 * C] + sums[3 * C :]) * v
        mid = cum[C // 2 - 1 : C // 2]
        end = cum[C - 1 : C]
        rel = cum - mid
        grow = jnp.exp(rel)
        shrink = jnp.exp(-rel)
        before_unit = jnp.exp(rel - log_step) * unit
        read_fwd = r * grow
        key_back = k * shrink
        erase_back = unit * rate * shrink
        grow_mid = jnp.exp(mid)
        grow_rest = jnp.exp(end - mid)
        grow_end = jnp.exp(end)
        left = jnp.concatenate([before_unit, read_fwd], axis=0).astype(BF16)
        by_key = dot_nt(left, bd(key_back))
        by_erase = dot_nt(left, bd(erase_back))
        yield
        key_both = jnp.concatenate(
            [jnp.where(strict, by_key[0:C], 0.0), jnp.where(inclusive, by_key[C:], 0.0)], axis=0
        ).astype(BF16)
        erase_past = jnp.where(strict, by_erase[0:C], 0.0)
        erase_read = jnp.where(inclusive, by_erase[C:], 0.0).astype(BF16)
        by_value = dot_nn(key_both, bd(vb))
        erase_tiled = tiled(erase_past)
        inv = eye - jnp.where(first_level, erase_past, 0.0)
        for n in range(len(LEVELS)):
            half = dot_nn(inv.astype(BF16), erase_tiled * level_ref[n])
            yield
            inv = inv - dot_nn(half.astype(BF16), bd(inv))
            yield
        inv_b = inv.astype(BF16)
        recalled = dot_nn(inv_b, bd(by_value[0:C]))
        carried_map = dot_nn(inv_b, bd(before_unit * grow_mid))
        yield
        recalled_b = recalled.astype(BF16)
        carried_b = carried_map.astype(BF16)
        local = by_value[C:] - dot_nn(erase_read, bd(recalled_b))
        from_start = (read_fwd * grow_mid - dot_nn(erase_read, bd(carried_b))).astype(BF16)
        key_end = (key_back * grow_rest).astype(BF16)
        erase_end = (erase_back * grow_rest).astype(BF16)
        gain = dot_tn(
            jnp.concatenate([vb, -recalled_b], axis=0),
            jnp.concatenate([key_end, erase_end], axis=0),
        )
        loss = dot_tn(carried_b, erase_end)
        yield
        result.append(
            (rows, local, from_start, diagonal_of(gain), loss.astype(BF16) * mask_ref[...], grow_end)
        )

    def group(g, _):
        results = [[] for _ in range(TOGETHER)]
        running = [chunk(g * TOGETHER + n, results[n]) for n in range(TOGETHER)]
        while running:
            left_over = []
            for one in running:
                try:
                    next(one)
                    left_over.append(one)
                except StopIteration:
                    pass
            running = left_over
        sm = sm_ref[...]
        for n in range(TOGETHER):
            rows, local, from_start, gain, loss, grow_end = results[n][0]
            sm_b = sm.astype(BF16)
            local_ref[rows, :] = local + dot_nt(from_start, bd(sm_b[0:C]))
            coef_ref[rows, :] = dot_nt(from_start, bd(sm_b[C:])).astype(BF16)
            sm = sm * grow_end - dot_nn(sm_b, loss)
            sm = jnp.concatenate([sm[0:C] + gain, sm[C:]], axis=0)
        sm_ref[...] = sm
        return 0

    lax.fori_loop(0, length // (C * TOGETHER), group, 0)

    def followed_by(sm, packet):
        prod = dot_nn(sm.astype(BF16), bd(packet[C:]))
        return jnp.concatenate([prod[0:C] + packet[0:C].astype(F32), prod[C:]], axis=0)

    own = sm_ref[...].astype(BF16)
    packet_y[...] = own
    recv_y[place_y] = own
    pl.semaphore_wait(barrier, n_y - 1 + n_z - 1)

    def copy_y(to, slot):
        return pltpu.make_async_remote_copy(
            src_ref=packet_y,
            dst_ref=recv_y.at[slot],
            send_sem=send_y_sem.at[to],
            recv_sem=recv_y_sem.at[slot],
            device_id={"sp_1": to},
            device_id_type=MESH,
        )

    for d in range(1, n_y):
        copy_y(lax.rem(place_y + d, n_y), place_y).start()
    for d in range(1, n_y):
        peer = lax.rem(place_y + n_y - d, n_y)
        copy_y(peer, peer).wait_recv()
    total = recv_y[0].astype(F32)
    inside = jnp.concatenate([jnp.zeros((C, width), F32), eye], axis=0)
    for m in range(1, n_y):
        inside = jnp.where(place_y == m, total, inside)
        total = followed_by(total, recv_y[m])
    packet_z[...] = total.astype(BF16)

    def copy_z(to, slot):
        return pltpu.make_async_remote_copy(
            src_ref=packet_z,
            dst_ref=recv_z.at[slot],
            send_sem=send_z_sem.at[to],
            recv_sem=recv_z_sem.at[slot],
            device_id={"sp_0": to},
            device_id_type=MESH,
        )

    for d in range(1, n_z):

        @pl.when(place_z + d < n_z)
        def _():
            copy_z(place_z + d, place_z).start()

    s_ref[...] = jnp.zeros((C, width), F32)
    for m in range(n_z - 1):

        @pl.when(m < place_z)
        def _():
            copy_z(m, m).wait_recv()
            arrived = recv_z[m]
            s_ref[...] = (
                dot_nn(s_ref[...].astype(BF16), bd(arrived[C:])) + arrived[0:C].astype(F32)
            )

    incoming = dot_nn(s_ref[...].astype(BF16), bd(inside[C:])) + inside[0:C]
    incoming_bd = bd(incoming)

    span = 4 * C
    for start in range(0, length, span):
        rows = pl.ds(start, span)
        outcome = local_ref[rows, :] + dot_nt(coef_ref[rows, :], incoming_bd)
        o_hi, o_lo = two_parts(outcome)
        centre = dot_nn(jnp.concatenate([o_hi, o_lo], axis=0), mask_ref[...])
        away = outcome - (centre[0:span] + centre[span:]) * (1.0 / C)
        a_hi, a_lo = two_parts(away * away)
        spread = dot_nn(jnp.concatenate([a_hi, a_lo], axis=0), mask_ref[...])
        spread = (spread[0:span] + spread[span:]) * (1.0 / C)
        normed = away * lax.rsqrt(spread + group_eps)
        out_ref[rows, :] = ((normed + extra_ref[rows, :]) * gate_ref[rows, :].astype(F32)).astype(
            BF16
        )

    for d in range(1, n_y):
        to = lax.rem(place_y + d, n_y)
        copy_y(to, to).wait_send()
    for d in range(1, n_z):

        @pl.when(place_z + d < n_z)
        def _():
            copy_z(place_z + d, place_z).wait_send()


def mixed_heads_of(r, k, v, gate, fd, afl, foff, sd, soff, scale):
    n_z, n_y = lax.axis_size("sp_0"), lax.axis_size("sp_1")
    length, width = r.shape
    vmem = pl.BlockSpec(memory_space=pltpu.VMEM)
    return pl.pallas_call(
        functools.partial(mixing_kernel, n_z, n_y),
        out_shape=jax.ShapeDtypeStruct((length, width), BF16),
        in_specs=[vmem] * 10,
        out_specs=vmem,
        scratch_shapes=[
            pltpu.VMEM((width, width), BF16),
            pltpu.VMEM((len(LEVELS), width, width), BF16),
            pltpu.VMEM((length, width), F32),
            pltpu.VMEM((length, width), BF16),
            pltpu.VMEM((length, width), F32),
            pltpu.VMEM((2 * C, width), F32),
            pltpu.VMEM((2 * C, width), BF16),
            pltpu.VMEM((n_y, 2 * C, width), BF16),
            pltpu.VMEM((2 * C, width), BF16),
            pltpu.VMEM((n_z, 2 * C, width), BF16),
            pltpu.VMEM((C, width), F32),
            pltpu.SemaphoreType.DMA((n_y,)),
            pltpu.SemaphoreType.DMA((n_y,)),
            pltpu.SemaphoreType.DMA((n_z,)),
            pltpu.SemaphoreType.DMA((n_z,)),
        ],
        compiler_params=pltpu.CompilerParams(
            collective_id=0, has_side_effects=True, vmem_limit_bytes=40 * 1024 * 1024
        ),
        cost_estimate=pl.CostEstimate(
            flops=40_000_000_000, bytes_accessed=3_000_000, transcendentals=0
        ),
        name="mixing",
    )(r, k, v, gate, fd, afl, foff[None, :], sd, soff[None, :], scale[None, :])


def sent_and_summed(shard, axis, dim):
    peers = lax.axis_size(axis)
    parts = lax.all_to_all(
        shard.reshape(peers, shard.shape[0] // peers, shard.shape[1]), axis, 0, 0, tiled=True
    )
    return jnp.sum(parts.astype(jnp.float32), axis=0)


def per_device(
    skip_stream,
    acceptance_signal,
    lookup_mapped,
    payload_mapped,
    result_switch,
    forget_dynamic_share,
    additive_forget_logarithm,
    forget_feature_offset,
    substitution_dynamic_share,
    substitution_feature_offset,
    diagonal_reward_scales,
    result_matrix,
    mlp_rescaler,
    switch_matrix,
    expand_matrix,
    contract_matrix,
):
    weights = jnp.concatenate([switch_matrix, expand_matrix, contract_matrix], axis=1)
    whole = lax.all_gather(weights, SP, axis=0, tiled=True)
    ff = switch_matrix.shape[1]
    gate_whole, up_whole, down_whole = whole[:, :ff], whole[:, ff : 2 * ff], whole[:, 2 * ff :]

    merged_attention = mixed_heads_of(
        acceptance_signal,
        lookup_mapped,
        payload_mapped,
        result_switch,
        forget_dynamic_share,
        additive_forget_logarithm,
        forget_feature_offset,
        substitution_dynamic_share,
        substitution_feature_offset,
        diagonal_reward_scales,
    )
    projected = sent_and_summed(
        jnp.dot(merged_attention, result_matrix, preferred_element_type=jnp.float32).astype(
            jnp.bfloat16
        ),
        "tp",
        0,
    ).astype(jnp.bfloat16)
    stream = skip_stream.astype(jnp.float32) + lax.optimization_barrier(projected).astype(
        jnp.float32
    )
    scale_rows = lax.rsqrt(jnp.mean(stream * stream, axis=-1, keepdims=True) + norm_eps)
    normed_rows = (stream * scale_rows * mlp_rescaler[None, :]).astype(jnp.bfloat16)
    whole_rows = lax.all_gather(normed_rows, "tp", axis=0, tiled=True)
    gate_act = jnp.dot(whole_rows, gate_whole, preferred_element_type=jnp.float32)
    up_act = jnp.dot(whole_rows, up_whole, preferred_element_type=jnp.float32)
    hidden = (jax.nn.silu(gate_act) * up_act).astype(jnp.bfloat16)
    ffn_out = lax.psum_scatter(
        lax.dot_general(
            hidden, down_whole, (((1,), (1,)), ((), ())), preferred_element_type=jnp.float32
        ).astype(jnp.bfloat16),
        "tp",
        scatter_dimension=0,
        tiled=True,
    )
    return (stream + half_step * lax.optimization_barrier(ffn_out).astype(jnp.float32)).astype(
        jnp.bfloat16
    )


def solution(mesh):
    torus = Mesh(mesh.devices.reshape(8, 4, mesh.shape["tp"]), ("sp_0", "sp_1", "tp"))
    in_specs = (
        P(SP_TP, None),
        P(SP, "tp"),
        P(SP, "tp"),
        P(SP, "tp"),
        P(SP, "tp"),
        P(SP, "tp"),
        P(SP, "tp"),
        P("tp"),
        P(SP, "tp"),
        P("tp"),
        P("tp"),
        P("tp", None),
        P(),
        P(SP, "tp"),
        P(SP, "tp"),
        P(SP, "tp"),
    )
    out_specs = P(SP_TP, None)
    return jax.shard_map(
        per_device, mesh=torus, in_specs=in_specs, out_specs=out_specs, check_vma=False
    )
```

time: 710 us -> 289 us (0.41)
  other arithmetic: 257 us -> 6.3 us
  blocking collectives: 123 us -> 43.6 us
  local copies, waits for them, and re-layouts: 76.8 us -> 9 us
  matrix products: 76.8 us -> 19.1 us
  Pallas kernels: 0 us -> 33 us
    another operation x50 -> x0, other arithmetic: 238 us -> none  [the longest x36 236 us: block_step(): jax.scipy.linalg.solve_triangular(erase_past, jnp.concatenate([recall_rhs...]
    all_gather x4 -> x0, blocking collectives: 63.5 us -> none  [carried_in(): lax.all_gather(part.astype(kind), axis)]
    dot_general x152 -> x2, matrix products: 64.9 us -> 12.5 us  [the longest x1 11.5 us: per_device(): lax.dot_general(hidden, down_whole, (((1,), (1,)), ((), ())), preferred_e...]
    dynamic_slice x72 -> x0, local copies, waits for them, and re-layouts: 46.8 us -> none  [per_device(): lax.scan(block_step, (zero_mats, identity_mats), (to_blocks(acceptance_li...]
    pallas_call x0 -> x1, Pallas kernels: none -> 33 us  [mixed_heads_of(): pl.pallas_call(functools.partial(mixing_kernel, n_z, n_y), out_shape=jax....]
    all_to_all x1, blocking collectives: 59.3 us -> 43.6 us  [sent_and_summed(): lax.all_to_all(shard.reshape(peers, shard.shape[0] // peers, shard.shape[...]
    another operation x4 -> x0, local copies, waits for them, and re-layouts: 8.03 us -> none  [to_blocks(): values.reshape(block_count, block_len, attention_groups, PER_GROUP_DIMS)]
where the time goes in v1:
time: 289 us; the launch traced here: 287 us
  waiting for transfers between devices  163 us (56%)
  blocking collectives  43.6 us (15%)
  Pallas kernels  33 us (11%)
  matrix products  19.1 us (7%)
  between operations  13.2 us (5%)
  local copies, waits for them, and re-layouts  9 us (3%)
  other arithmetic  6.3 us (2%)
    all_gather x1, waiting for transfers between devices, per_device(): whole = lax.all_gather(weights, SP, axis=0, tiled=True)  96.7 us
    all_to_all x1, blocking collectives, sent_and_summed(): lax.all_to_all(shard.reshape(peers, shard.shape[0] // peers, shard.shape[...  43.6 us
    reduce_scatter x1, waiting for transfers between devices, per_device(): lax.psum_scatter(lax.dot_general(hidden, down_whole, (((1,), (1,)), ((),...  33.9 us
    pallas_call x1, Pallas kernels, mixed_heads_of(): pl.pallas_call(functools.partial(mixing_kernel, n_z, n_y), out_shape=jax....  33 us
    all_gather x1, waiting for transfers between devices, per_device(): whole_rows = lax.all_gather(normed_rows, 'tp', axis=0, tiled=True)  32 us
    dot_general x1, matrix products, per_device(): lax.dot_general(hidden, down_whole, (((1,), (1,)), ((), ())), preferred_e...  11.5 us
    unnamed x31, local copies, waits for them, and re-layouts  9 us
    dot_general x1, matrix products, per_device(): jnp.dot(whole_rows, gate_whole, preferred_element_type=jnp.float32)  6.56 us
  transfers between devices with their start and end apart: 3, of which 3 were waited for; matrix products, arithmetic and copies ran while one was open for 0% of the time, Pallas kernels for 0%

profile of v1, /device:TPU:1, one launch (start us, length us, event | category | flops | bytes accessed | tf_op | source)
XLA Modules:
  0.0 287.1 jit_solution(691345789440403118)
XLA Ops:
  6.5 1.0 copy.17.afl_ref
  7.5 1.0 copy-done.1
  8.5 1.0 copy-done.2
  9.5 1.0 copy-done.3
  10.5 1.0 copy-done.4
  11.5 1.0 copy-done.5
  12.5 1.0 copy-done.6
  13.5 0.7 copy-done.7
  14.2 0.7 copy-done.8
  14.9 0.7 copy-done.9
  15.5 33.0 %mixing.1 = bf16[768,256]{1,0:T(8,128)(2,1)S(1)} custom-call(bf16[768,256]{1,0:T(8,128)(2,1)S(1)} %copy-done.1, bf16[768,256]{1,0:T(8,128)(2,1)S(1)} %copy-done.2, bf16[768,256]{1,0:T(8,128)(2,1)S(1)} %copy-done.3, bf16[768,256]{1,0:T(8,128)(2,1)S(1)} %copy-done.4, bf16[768,256]{1,0:T(8,128)(2,1)S(1)} %copy-done.5, f32[768,4]{1,0:T(8,128)S(1)} %copy.17.afl_ref, ...), custom_call_target="tpu_custom_call" | custom-call | flops 40000000000 | bytes 3000000 | tf_op jit(solution)/shard_map/mixing/pallas_call | solution.py:315
  48.6 1.0 convolution_convert_fusion.1
  49.5 43.6 %all_to_all.5 = bf16[8,96,2048]{2,1,0:T(8,128)(2,1)} all-to-all(bf16[8,96,2048]{2,1,0:T(8,128)(2,1)S(1)} %bitcast.11), channel_id=1, replica_groups=mesh['sp_0'=8,'sp_1'=4,'tp'=8] {'tp'}, dimensions={0} | all-to-all | bytes 6291456 | tf_op jit(solution)/shard_map/all_to_all | solution.py:349
  93.1 2.5 reduce_sum.21
  95.7 0.2 multiply_reduce_fusion
  95.9 0.9 multiply_convert_fusion.1
  97.0 0.7 pad_maximum_fusion
  97.7 0.2 reduce-scatter.2.cloned.1.call-start
  97.9 32.0 %all-gather.3.cloned.1.call-done = bf16[768,2048]{1,0:T(8,128)(2,1)} async-done(((bf16[96,2048]{1,0:T(8,128)(2,1)}), bf16[768,2048]{1,0:T(8,128)(2,1)}) %all-gather.3.cloned.1.call-update) | async-done | bytes 3145744 | tf_op jit(solution)/shard_map/all_gather | solution.py:402
  129.9 96.7 %all-gather.5.cloned.1.call-done = bf16[2048,1920]{1,0:T(8,128)(2,1)} async-done(((bf16[64,1920]{1,0:T(8,128)(2,1)}), bf16[2048,1920]{1,0:T(8,128)(2,1)}) %all-gather.5.cloned.1.call-update) | async-done | bytes 7864336 | tf_op jit(solution)/shard_map/all_gather | solution.py:374
  226.6 6.6 %fusion.3 = f32[768,640]{1,0:T(8,128)} fusion(bf16[768,2048]{1,0:T(8,128)(2,1)} %all-gather.3.cloned.1.call-done, bf16[2048,1920]{1,0:T(8,128)(2,1)} %all-gather.5.cloned.1.call-done), kind=kOutput, calls=%fused_computation.5 | convolution fusion | flops 2013265920 | bytes 7733248 | tf_op jit(solution)/shard_map/dot_general | solution.py:403
  233.2 11.5 %convolution_convert_fusion = bf16[768,2048]{1,0:T(8,128)(2,1)} fusion(bf16[2048,1920]{1,0:T(8,128)(2,1)} %all-gather.5.cloned.1.call-done, f32[768,640]{1,0:T(8,128)} %fusion.3, bf16[768,2048]{1,0:T(8,128)(2,1)} %all-gather.3.cloned.1.call-done), kind=kOutput, calls=%fused_computation | convolution fusion | flops 4031053824 | bytes 13500416 | tf_op jit(solution)/shard_map/dot_general | solution.py:407
  244.8 33.9 %reduce-scatter.2.cloned.1.call-done = bf16[96,2048]{1,0:T(8,128)(2,1)} async-done(((bf16[768,2048]{1,0:T(8,128)(2,1)}), bf16[96,2048]{1,0:T(8,128)(2,1)}) %reduce-scatter.2.cloned.1.call-update) | async-done | bytes 393232 | tf_op jit(solution)/shard_map/reduce_scatter | solution.py:406
  278.6 1.9 add_convert_fusion
  (27 shorter events, 0.1 us)
Async XLA Ops:
  6.5 42.0 %copy-start = (bf16[256,2048]{1,0:T(8,128)(2,1)S(1)}, bf16[256,2048]{1,0:T(8,128)(2,1)}, u32[]{:S(2)}) copy-start(bf16[256,2048]{1,0:T(8,128)(2,1)} %param.27) | copy-start | bytes 3145732
  6.5 123.4 %all-gather.3.cloned.1.call-start = ((), (), s32[]{:S(2)}) async-start(), calls=%async_computation.2 | async-start | bytes 3538944 | tf_op jit(solution)/shard_map/all_gather | solution.py:402
  7.5 1.0 copy-start.1
  8.5 1.0 copy-start.2
  9.5 1.0 copy-start.3
  10.5 1.0 copy-start.4
  11.5 1.0 copy-start.5
  12.5 1.0 copy-start.6
  13.5 0.7 copy-start.7
  14.2 0.7 copy-start.8
  14.9 0.7 copy-start.9
  93.1 2.6 copy-start.10
  93.1 2.8 copy-start.14
  93.1 3.8 %copy-start.11 = (bf16[64,640]{1,0:T(8,128)(2,1)S(1)}, bf16[64,640]{1,0:T(8,128)(2,1)}, u32[]{:S(2)}) copy-start(bf16[64,640]{1,0:T(8,128)(2,1)} %param.31) | copy-start | bytes 245764
  93.1 3.8 %copy-start.12 = (bf16[64,640]{1,0:T(8,128)(2,1)S(1)}, bf16[64,640]{1,0:T(8,128)(2,1)}, u32[]{:S(2)}) copy-start(bf16[64,640]{1,0:T(8,128)(2,1)} %param.30) | copy-start | bytes 245764
  93.1 3.8 %copy-start.13 = (bf16[64,640]{1,0:T(8,128)(2,1)S(1)}, bf16[64,640]{1,0:T(8,128)(2,1)}, u32[]{:S(2)}) copy-start(bf16[64,640]{1,0:T(8,128)(2,1)} %param.29) | copy-start | bytes 245764
  96.9 129.8 %all-gather.5.cloned.1.call-start = ((), (), s32[]{:S(2)}) async-start(), calls=%async_computation.3 | async-start | bytes 8110080 | tf_op jit(solution)/shard_map/all_gather | solution.py:374
  97.7 181.0 %reduce-scatter.2.cloned.1.call-start = ((), (), s32[]{:S(2)}) async-start(), calls=%async_computation.4 | async-start | bytes 3538944 | tf_op jit(solution)/shard_map/reduce_scatter | solution.py:406
Sparse Core Ops, SparseCore 0:
  97.0 32.9 all-gather.2
  132.5 94.0 all-gather.4
  244.9 33.7 reduce-scatter.1

commit v2 on v1

--- a/solution.py
+++ b/solution.py
@@ -42,20 +42,328 @@
     return high, (x - high.astype(F32)).astype(BF16)
 
 
+ROWS = 96
+HALF = 1024
+
+
+def ring_places():
+    tp = lax.axis_index("tp")
+    chip, core = tp // 2, tp % 2
+    right = lax.rem(chip + 1, 4) * 2 + core
+    left = lax.rem(chip + 3, 4) * 2 + core
+    sibling = chip * 2 + 1 - core
+    return chip, core, right, left, sibling
+
+
+def remote(src, dst, send_sem, recv_sem, to):
+    return pltpu.make_async_remote_copy(
+        src_ref=src,
+        dst_ref=dst,
+        send_sem=send_sem,
+        recv_sem=recv_sem,
+        device_id={"tp": to},
+        device_id_type=MESH,
+    )
+
+
+class RingSum:
+    def __init__(self, part, sib, pair, relay, arrived, sems):
+        self.part, self.sib, self.pair, self.relay, self.arrived = part, sib, pair, relay, arrived
+        self.sib_send, self.sib_recv, self.send, self.recv = sems
+        self.chip, self.core, self.right, self.left, self.sibling = ring_places()
+        self.own = pl.ds(pl.multiple_of(self.core * ROWS, ROWS), ROWS)
+        self.other = pl.ds(pl.multiple_of((1 - self.core) * ROWS, ROWS), ROWS)
+
+    def to_sibling(self, d):
+        return remote(
+            self.part.at[d, :, self.other, :],
+            self.sib.at[d],
+            self.sib_send.at[d],
+            self.sib_recv.at[d],
+            self.sibling,
+        )
+
+    def hop(self, n):
+        src, dst, to = (
+            (self.pair.at[2, 0], self.relay.at[0], self.right),
+            (self.pair.at[2, 1], self.relay.at[1], self.left),
+            (self.pair.at[1, 1], self.arrived.at[0, 1], self.right),
+            (self.pair.at[3, 0], self.arrived.at[1, 0], self.left),
+            (self.pair.at[1, 0], self.arrived.at[0, 0], self.right),
+            (self.pair.at[3, 1], self.arrived.at[1, 1], self.left),
+        )[n]
+        return remote(src, dst, self.send.at[n], self.recv.at[n], to)
+
+    def produced(self, d):
+        self.to_sibling(d).start()
+
+    def summed(self, d, h):
+        return self.part[d, h, self.own, :].astype(F32) + self.sib[d, h].astype(F32)
+
+    def pass_on(self, d):
+        self.to_sibling(d).wait_recv()
+        if d == 2:
+            self.pair[2, 0] = self.summed(2, 0).astype(BF16)
+            self.hop(0).start()
+            self.pair[2, 1] = self.summed(2, 1).astype(BF16)
+            self.hop(1).start()
+        if d == 1:
+            self.pair[1, 1] = self.summed(1, 1).astype(BF16)
+            self.hop(2).start()
+        if d == 3:
+            self.pair[3, 0] = self.summed(3, 0).astype(BF16)
+            self.hop(3).start()
+
+    def pass_relayed(self):
+        self.hop(0).wait_recv()
+        self.pair[1, 0] = (self.summed(1, 0) + self.relay[0].astype(F32)).astype(BF16)
+        self.hop(4).start()
+        self.hop(1).wait_recv()
+        self.pair[3, 1] = (self.summed(3, 1) + self.relay[1].astype(F32)).astype(BF16)
+        self.hop(5).start()
+
+    def arrive(self):
+        for n in (2, 3, 4, 5):
+            self.hop(n).wait_recv()
+
+    def result(self, h):
+        return (
+            self.summed(0, h)
+            + self.arrived[0, h].astype(F32)
+            + self.arrived[1, h].astype(F32)
+        )
+
+    def drain(self):
+        for d in range(4):
+            self.to_sibling(d).wait_send()
+        for n in range(6):
+            self.hop(n).wait_send()
+
+
+RING_SUM_SCRATCH = [
+    pltpu.VMEM((4, 2, 2 * ROWS, HALF), BF16),
+    pltpu.VMEM((4, 2, ROWS, HALF), BF16),
+    pltpu.VMEM((4, 2, ROWS, HALF), BF16),
+    pltpu.VMEM((2, ROWS, HALF), BF16),
+    pltpu.VMEM((2, 2, ROWS, HALF), BF16),
+    pltpu.SemaphoreType.DMA((4,)),
+    pltpu.SemaphoreType.DMA((4,)),
+    pltpu.SemaphoreType.DMA((6,)),
+    pltpu.SemaphoreType.DMA((6,)),
+]
+
+
+def greet_ring(barrier):
+    _, _, right, left, sibling = ring_places()
+    for to in (right, left, sibling):
+        pl.semaphore_signal(barrier, inc=1, device_id={"tp": to}, device_id_type=MESH)
+
+
+def feed_forward_kernel(
+    rows_in_ref,
+    stream_ref,
+    gate_up_hbm,
+    down_hbm,
+    out_ref,
+    gate_up_ref,
+    down_ref,
+    rows_ref,
+    hidden_ref,
+    part_ref,
+    sib_ref,
+    pair_ref,
+    relay_ref,
+    arrived_ref,
+    sib_send,
+    sib_recv,
+    hop_send,
+    hop_recv,
+    load_sem,
+    row_send,
+    row_recv,
+    side_send,
+    side_recv,
+):
+    barrier = pltpu.get_barrier_semaphore()
+    greet_ring(barrier)
+    chip, core, right, left, sibling = ring_places()
+    load_gate_up = pltpu.make_async_copy(gate_up_hbm, gate_up_ref, load_sem.at[0])
+    load_down = pltpu.make_async_copy(down_hbm, down_ref, load_sem.at[1])
+    load_gate_up.start()
+    load_down.start()
+    here = pl.ds(pl.multiple_of(core * ROWS, ROWS), ROWS)
+    there = pl.ds(pl.multiple_of((1 - core) * ROWS, ROWS), ROWS)
+
+    def chip_at(d):
+        return lax.rem(chip + d, 4)
+
+    rows_ref[chip, :, here, :] = rows_in_ref[...]
+    pl.semaphore_wait(barrier, 3)
+
+    def hop(n):
+        d, h, to = (
+            (0, 0, right),
+            (0, 1, left),
+            (0, 1, right),
+            (0, 0, left),
+            (3, 0, right),
+            (1, 1, left),
+        )[n]
+        block = rows_ref.at[chip_at(d), h, here, :]
+        return remote(block, block, row_send.at[n], row_recv.at[n], to)
+
+    def arrival(n):
+        d, h = ((3, 0), (1, 1), (3, 1), (1, 0), (2, 0), (2, 1))[n]
+        block = rows_ref.at[chip_at(d), h, here, :]
+        return remote(block, block, row_send.at[n], row_recv.at[n], sibling)
+
+    def side(n):
+        d, h = ((0, 0), (0, 1), (1, 0), (1, 1), (3, 0), (3, 1), (2, 0), (2, 1))[n]
+        block = rows_ref.at[chip_at(d), h, here, :]
+        return remote(block, block, side_send.at[n], side_recv.at[n], sibling)
+
+    def side_arrival(n):
+        d, h = ((0, 0), (0, 1), (1, 0), (1, 1), (3, 0), (3, 1), (2, 0), (2, 1))[n]
+        block = rows_ref.at[chip_at(d), h, there, :]
+        return remote(block, block, side_send.at[n], side_recv.at[n], sibling)
+
+    for n in range(4):
+        hop(n).start()
+    side(0).start()
+    side(1).start()
+
+    ring = RingSum(
+        part_ref,
+        sib_ref,
+        pair_ref,
+        relay_ref,
+        arrived_ref,
+        (sib_send, sib_recv, hop_send, hop_recv),
+    )
+    ff_half = hidden_ref.shape[1]
+
+    def produce(d):
+        block = chip_at(d)
+        x = [rows_ref[block, 0], rows_ref[block, 1]]
+        for n in range(ff_half // 128):
+            cols = pl.ds(256 * n, 256)
+            both = dot_nn(x[0], gate_up_ref[0:HALF, cols]) + dot_nn(x[1], gate_up_ref[HALF:, cols])
+            gate_act, up_act = both[:, :128], both[:, 128:]
+            hidden_ref[:, pl.ds(128 * n, 128)] = (
+                gate_act * jax.nn.sigmoid(gate_act) * up_act
+            ).astype(BF16)
+        hidden = hidden_ref[...]
+        for h in range(2):
+            for n in range(HALF // 256):
+                part_ref[d, h, :, pl.ds(256 * n, 256)] = dot_nt(
+                    hidden, down_ref[pl.ds(h * HALF + 256 * n, 256), :]
+                ).astype(BF16)
+        ring.produced(d)
+
+    side_arrival(0).wait_recv()
+    side_arrival(1).wait_recv()
+    load_gate_up.wait()
+    load_down.wait()
+    produce(0)
+    arrival(0).wait_recv()
+    hop(4).start()
+    side(4).start()
+    arrival(1).wait_recv()
+    hop(5).start()
+    side(3).start()
+    arrival(2).wait_recv()
+    side(5).start()
+    arrival(3).wait_recv()
+    side(2).start()
+    side_arrival(4).wait_recv()
+    side_arrival(5).wait_recv()
+    produce(3)
+    side_arrival(2).wait_recv()
+    side_arrival(3).wait_recv()
+    arrival(4).wait_recv()
+    side(6).start()
+    arrival(5).wait_recv()
+    side(7).start()
+    ring.pass_on(3)
+    produce(1)
+    ring.pass_on(1)
+    side_arrival(6).wait_recv()
+    side_arrival(7).wait_recv()
+    produce(2)
+    ring.pass_on(2)
+    ring.pass_relayed()
+    ring.to_sibling(0).wait_recv()
+    ring.arrive()
+    for h in range(2):
+        out_ref[:, pl.ds(h * HALF, HALF)] = (
+            stream_ref[:, pl.ds(h * HALF, HALF)] + half_step * ring.result(h)
+        ).astype(BF16)
+    ring.drain()
+    for n in range(6):
+        hop(n).wait_send()
+    for n in range(8):
+        side(n).wait_send()
+
+
+def feed_forward(rows, stream, gate_up, down):
+    vmem = pl.BlockSpec(memory_space=pltpu.VMEM)
+    hbm = pl.BlockSpec(memory_space=pl.ANY)
+    ff = down.shape[1]
+    return pl.pallas_call(
+        feed_forward_kernel,
+        out_shape=jax.ShapeDtypeStruct((ROWS, 2 * HALF), BF16),
+        in_specs=[vmem, vmem, hbm, hbm],
+        out_specs=vmem,
+        scratch_shapes=[
+            pltpu.VMEM(gate_up.shape, BF16),
+            pltpu.VMEM(down.shape, BF16),
+            pltpu.VMEM((4, 2, 2 * ROWS, HALF), BF16),
+            pltpu.VMEM((2 * ROWS, ff), BF16),
+        ]
+        + RING_SUM_SCRATCH
+        + [
+            pltpu.SemaphoreType.DMA((2,)),
+            pltpu.SemaphoreType.DMA((6,)),
+            pltpu.SemaphoreType.DMA((6,)),
+            pltpu.SemaphoreType.DMA((8,)),
+            pltpu.SemaphoreType.DMA((8,)),
+        ],
+        compiler_params=pltpu.CompilerParams(
+            collective_id=1, has_side_effects=True, vmem_limit_bytes=56 * 1024 * 1024
+        ),
+        cost_estimate=pl.CostEstimate(
+            flops=20_000_000_000, bytes_accessed=8_000_000, transcendentals=0
+        ),
+        name="feed_forward",
+    )(rows, stream, gate_up, down)
+
+
 def mixing_kernel(
     n_z,
     n_y,
+    r_hbm,
+    k_hbm,
+    v_hbm,
+    gate_hbm,
+    fd_hbm,
+    afl_ref,
+    foff_ref,
+    sd_hbm,
+    soff_ref,
+    scale_ref,
+    skip_ref,
+    matrix_hbm,
+    gain_ref,
+    rows_out_ref,
+    stream_ref,
     r_ref,
     k_ref,
     v_ref,
     gate_ref,
     fd_ref,
-    afl_ref,
-    foff_ref,
     sd_ref,
-    soff_ref,
-    scale_ref,
-    out_ref,
+    matrix_ref,
+    load_sem,
     mask_ref,
     level_ref,
     local_ref,
@@ -71,13 +379,31 @@
     recv_y_sem,
     send_z_sem,
     recv_z_sem,
+    *ring_refs,
 ):
     length, width = r_ref.shape
     heads = width // C
     place_z = lax.axis_index("sp_0")
     place_y = lax.axis_index("sp_1")
 
+    loads = [
+        pltpu.make_async_copy(src, dst, load_sem.at[n])
+        for n, (src, dst) in enumerate(
+            (
+                (r_hbm, r_ref),
+                (k_hbm, k_ref),
+                (v_hbm, v_ref),
+                (fd_hbm, fd_ref),
+                (sd_hbm, sd_ref),
+                (gate_hbm, gate_ref),
+                (matrix_hbm, matrix_ref),
+            )
+        )
+    ]
+    for load in loads:
+        load.start()
     barrier = pltpu.get_barrier_semaphore()
+    greet_ring(barrier)
     for d in range(1, n_y):
         pl.semaphore_signal(
             barrier, inc=1, device_id={"sp_1": lax.rem(place_y + d, n_y)}, device_id_type=MESH
@@ -220,6 +546,8 @@
         sm_ref[...] = sm
         return 0
 
+    for load in loads[:5]:
+        load.wait()
     lax.fori_loop(0, length // (C * TOGETHER), group, 0)
 
     def followed_by(sm, packet):
@@ -229,7 +557,7 @@
     own = sm_ref[...].astype(BF16)
     packet_y[...] = own
     recv_y[place_y] = own
-    pl.semaphore_wait(barrier, n_y - 1 + n_z - 1)
+    pl.semaphore_wait(barrier, n_y - 1 + n_z - 1 + 3)
 
     def copy_y(to, slot):
         return pltpu.make_async_remote_copy(
@@ -282,10 +610,15 @@
 
     incoming = dot_nn(s_ref[...].astype(BF16), bd(inside[C:])) + inside[0:C]
     incoming_bd = bd(incoming)
-
-    span = 4 * C
-    for start in range(0, length, span):
-        rows = pl.ds(start, span)
+    loads[5].wait()
+    loads[6].wait()
+
+    span = 2 * ROWS
+    ring = RingSum(*ring_refs[:5], ring_refs[5:])
+
+    def produce(d):
+        start = lax.rem(ring.chip + d, 4) * span
+        rows = pl.ds(pl.multiple_of(start, span), span)
         outcome = local_ref[rows, :] + dot_nt(coef_ref[rows, :], incoming_bd)
         o_hi, o_lo = two_parts(outcome)
         centre = dot_nn(jnp.concatenate([o_hi, o_lo], axis=0), mask_ref[...])
@@ -294,9 +627,36 @@
         spread = dot_nn(jnp.concatenate([a_hi, a_lo], axis=0), mask_ref[...])
         spread = (spread[0:span] + spread[span:]) * (1.0 / C)
         normed = away * lax.rsqrt(spread + group_eps)
-        out_ref[rows, :] = ((normed + extra_ref[rows, :]) * gate_ref[rows, :].astype(F32)).astype(
-            BF16
-        )
+        mixed = ((normed + extra_ref[rows, :]) * gate_ref[rows, :].astype(F32)).astype(BF16)
+        for h in range(2):
+            for n in range(HALF // 256):
+                ring.part[d, h, :, pl.ds(256 * n, 256)] = dot_nn(
+                    mixed, matrix_ref[:, pl.ds(h * HALF + 256 * n, 256)]
+                ).astype(BF16)
+        ring.produced(d)
+
+    produce(2)
+    produce(1)
+    ring.pass_on(2)
+    produce(3)
+    ring.pass_on(1)
+    produce(0)
+    ring.pass_on(3)
+    ring.pass_relayed()
+    ring.to_sibling(0).wait_recv()
+    ring.arrive()
+    squares = jnp.zeros((ROWS, 1), F32)
+    for h in range(2):
+        cols = pl.ds(h * HALF, HALF)
+        stream = skip_ref[:, cols].astype(F32) + ring.result(h)
+        stream_ref[:, cols] = stream
+        squares = squares + jnp.sum(stream * stream, axis=1, keepdims=True)
+    scale_rows = lax.rsqrt(squares * (1.0 / (2 * HALF)) + norm_eps)
+    for h in range(2):
+        cols = pl.ds(h * HALF, HALF)
+        rows_out_ref[h] = (stream_ref[:, cols] * scale_rows * gain_ref[:, cols]).astype(BF16)
+    ring.drain()
+
 
     for d in range(1, n_y):
         to = lax.rem(place_y + d, n_y)
@@ -308,16 +668,23 @@
             copy_z(place_z + d, place_z).wait_send()
 
 
-def mixed_heads_of(r, k, v, gate, fd, afl, foff, sd, soff, scale):
+def mixed_rows_of(r, k, v, gate, fd, afl, foff, sd, soff, scale, skip, matrix, gain):
     n_z, n_y = lax.axis_size("sp_0"), lax.axis_size("sp_1")
     length, width = r.shape
     vmem = pl.BlockSpec(memory_space=pltpu.VMEM)
+    hbm = pl.BlockSpec(memory_space=pl.ANY)
     return pl.pallas_call(
         functools.partial(mixing_kernel, n_z, n_y),
-        out_shape=jax.ShapeDtypeStruct((length, width), BF16),
-        in_specs=[vmem] * 10,
-        out_specs=vmem,
-        scratch_shapes=[
+        out_shape=(
+            jax.ShapeDtypeStruct((2, ROWS, HALF), BF16),
+            jax.ShapeDtypeStruct((ROWS, 2 * HALF), F32),
+        ),
+        in_specs=[hbm] * 5 + [vmem, vmem, hbm, vmem, vmem, vmem, hbm, vmem],
+        out_specs=(vmem, vmem),
+        scratch_shapes=[pltpu.VMEM((length, width), BF16)] * 6
+        + [
+            pltpu.VMEM((width, 2 * HALF), BF16),
+            pltpu.SemaphoreType.DMA((7,)),
             pltpu.VMEM((width, width), BF16),
             pltpu.VMEM((len(LEVELS), width, width), BF16),
             pltpu.VMEM((length, width), F32),
@@ -333,23 +700,19 @@
             pltpu.SemaphoreType.DMA((n_y,)),
             pltpu.SemaphoreType.DMA((n_z,)),
             pltpu.SemaphoreType.DMA((n_z,)),
-        ],
+        ]
+        + RING_SUM_SCRATCH,
         compiler_params=pltpu.CompilerParams(
-            collective_id=0, has_side_effects=True, vmem_limit_bytes=40 * 1024 * 1024
+            collective_id=0, has_side_effects=True, vmem_limit_bytes=56 * 1024 * 1024
         ),
         cost_estimate=pl.CostEstimate(
             flops=40_000_000_000, bytes_accessed=3_000_000, transcendentals=0
         ),
         name="mixing",
-    )(r, k, v, gate, fd, afl, foff[None, :], sd, soff[None, :], scale[None, :])
-
-
-def sent_and_summed(shard, axis, dim):
-    peers = lax.axis_size(axis)
-    parts = lax.all_to_all(
-        shard.reshape(peers, shard.shape[0] // peers, shard.shape[1]), axis, 0, 0, tiled=True
+    )(
+        r, k, v, gate, fd, afl, foff[None, :], sd, soff[None, :], scale[None, :], skip, matrix,
+        gain[None, :],
     )
-    return jnp.sum(parts.astype(jnp.float32), axis=0)
 
 
 def per_device(
@@ -370,12 +733,14 @@
     expand_matrix,
     contract_matrix,
 ):
-    weights = jnp.concatenate([switch_matrix, expand_matrix, contract_matrix], axis=1)
-    whole = lax.all_gather(weights, SP, axis=0, tiled=True)
-    ff = switch_matrix.shape[1]
-    gate_whole, up_whole, down_whole = whole[:, :ff], whole[:, ff : 2 * ff], whole[:, 2 * ff :]
-
-    merged_attention = mixed_heads_of(
+    depth, ff = switch_matrix.shape
+    paired = jnp.stack(
+        [switch_matrix.reshape(depth, -1, 128), expand_matrix.reshape(depth, -1, 128)], axis=2
+    ).reshape(depth, 2 * ff)
+    with jax.named_scope("weights"):
+        gate_up = lax.all_gather(paired, SP, axis=0, tiled=True)
+        down = lax.all_gather(contract_matrix, SP, axis=0, tiled=True)
+    rows, stream = mixed_rows_of(
         acceptance_signal,
         lookup_mapped,
         payload_mapped,
@@ -386,34 +751,11 @@
         substitution_dynamic_share,
         substitution_feature_offset,
         diagonal_reward_scales,
+        skip_stream,
+        result_matrix,
+        mlp_rescaler,
     )
-    projected = sent_and_summed(
-        jnp.dot(merged_attention, result_matrix, preferred_element_type=jnp.float32).astype(
-            jnp.bfloat16
-        ),
-        "tp",
-        0,
-    ).astype(jnp.bfloat16)
-    stream = skip_stream.astype(jnp.float32) + lax.optimization_barrier(projected).astype(
-        jnp.float32
-    )
-    scale_rows = lax.rsqrt(jnp.mean(stream * stream, axis=-1, keepdims=True) + norm_eps)
-    normed_rows = (stream * scale_rows * mlp_rescaler[None, :]).astype(jnp.bfloat16)
-    whole_rows = lax.all_gather(normed_rows, "tp", axis=0, tiled=True)
-    gate_act = jnp.dot(whole_rows, gate_whole, preferred_element_type=jnp.float32)
-    up_act = jnp.dot(whole_rows, up_whole, preferred_element_type=jnp.float32)
-    hidden = (jax.nn.silu(gate_act) * up_act).astype(jnp.bfloat16)
-    ffn_out = lax.psum_scatter(
-        lax.dot_general(
-            hidden, down_whole, (((1,), (1,)), ((), ())), preferred_element_type=jnp.float32
-        ).astype(jnp.bfloat16),
-        "tp",
-        scatter_dimension=0,
-        tiled=True,
-    )
-    return (stream + half_step * lax.optimization_barrier(ffn_out).astype(jnp.float32)).astype(
-        jnp.bfloat16
-    )
+    return feed_forward(rows, stream, gate_up, down)
 
 
 def solution(mesh):

time: 289 us -> 228 us (0.79)
  Pallas kernels: 33 us -> 89.7 us
  waiting for transfers between devices: 163 us -> 118 us
  blocking collectives: 43.6 us -> 0 us
  matrix products: 19.1 us -> 0 us
  other arithmetic: 6.3 us -> 0.06 us
    pallas_call x1 -> x2, Pallas kernels: 33 us -> 89.7 us  [the longest x1 47.2 us: mixed_rows_of(): pl.pallas_call(functools.partial(mixing_kernel, n_z, n_y), out_shape=(jax...]
    all_to_all x1 -> x0, blocking collectives: 43.6 us -> none  [sent_and_summed(): lax.all_to_all(shard.reshape(peers, shard.shape[0] // peers, shard.shape[...]
    reduce_scatter x1 -> x0, waiting for transfers between devices: 33.9 us -> none  [per_device(): lax.psum_scatter(lax.dot_general(hidden, down_whole, (((1,), (1,)), ((),...]
    dot_general x3 -> x0, matrix products: 19.1 us -> none  [the longest x1 11.5 us: per_device(): lax.dot_general(hidden, down_whole, (((1,), (1,)), ((), ())), preferred_e...]
    all_gather x2, waiting for transfers between devices: 129 us -> 117 us  [the longest x1 85.6 us: per_device(): gate_up = lax.all_gather(paired, SP, axis=0, tiled=True)]
    unnamed x31 -> x2, local copies, waits for them, and re-layouts: 9 us -> 3.41 us
  transfers between devices with their start and end apart: 3 -> 2, of which waited for: 3 -> 2; matrix products, arithmetic and copies ran while one was open for 0% -> 2% of each run, Pallas kernels for 0% -> 21%
where the time goes in v2:
time: 228 us; the launch traced here: 227 us
  waiting for transfers between devices  118 us (52%)
  Pallas kernels  89.7 us (39%)
  between operations  13.4 us (6%)
  local copies, waits for them, and re-layouts  6.35 us (3%)
    all_gather x1, waiting for transfers between devices, per_device(): gate_up = lax.all_gather(paired, SP, axis=0, tiled=True)  85.6 us
    pallas_call x1, Pallas kernels, mixed_rows_of(): pl.pallas_call(functools.partial(mixing_kernel, n_z, n_y), out_shape=(jax...  47.2 us
    pallas_call x1, Pallas kernels, feed_forward(): pl.pallas_call(feed_forward_kernel, out_shape=jax.ShapeDtypeStruct((ROWS,...  42.5 us
    all_gather x1, waiting for transfers between devices, per_device(): down = lax.all_gather(contract_matrix, SP, axis=0, tiled=True)  31.6 us
  transfers between devices with their start and end apart: 2, of which 2 were waited for; matrix products, arithmetic and copies ran while one was open for 2% of the time, Pallas kernels for 21%

profile of v2, /device:TPU:1, one launch (start us, length us, event | category | flops | bytes accessed | tf_op | source)
XLA Modules:
  0.0 227.5 jit_solution(17748760714486319741)
XLA Ops:
  6.5 0.0 all-gather.5.cloned.1.call-start
  6.5 0.7 all-gather.5.cloned.1.call-update
  7.3 0.0 all-gather.3.cloned.1.call-start
  7.3 1.0 stack_reshape.6
  8.3 1.0 stack_reshape.7
  9.3 0.1 pad_maximum_fusion
  9.4 0.2 copy.21
  9.6 0.8 reshape.3
  10.3 0.0 all-gather.3.cloned.1.call-update
  10.3 1.6 copy.20.afl_ref
  12.0 47.2 %mixing.1 = (bf16[2,96,1024]{2,1,0:T(8,128)(2,1)}, f32[96,2048]{1,0:T(8,128)}) custom-call(bf16[768,256]{1,0:T(8,128)(2,1)} %r_hbm.1, bf16[768,256]{1,0:T(8,128)(2,1)} %k_hbm.1, bf16[768,256]{1,0:T(8,128)(2,1)} %v_hbm.1, bf16[768,256]{1,0:T(8,128)(2,1)} %gate_hbm.1, bf16[768,256]{1,0:T(8,128)(2,1)} %fd_hbm.1, f32[768,4]{1,0:T(8,128)} %copy.20.afl_ref, ...), custom_call_target="tpu_custom_call" | custom-call | flops 40000000000 | bytes 3000000 | tf_op jit(solution)/shard_map/mixing/pallas_call | solution.py:676
  59.2 31.6 %all-gather.5.cloned.1.call-done.down_hbm = bf16[2048,640]{1,0:T(8,128)(2,1)} async-done(((bf16[64,640]{1,0:T(8,128)(2,1)}), bf16[2048,640]{1,0:T(8,128)(2,1)}) %all-gather.5.cloned.1.call-update) | async-done | bytes 2621456 | tf_op jit(solution)/shard_map/weights/all_gather | solution.py:742
  90.8 85.6 %all-gather.3.cloned.1.call-done.gate_up_hbm = bf16[2048,1280]{1,0:T(8,128)(2,1)} async-done(((bf16[64,1280]{1,0:T(8,128)(2,1)}), bf16[2048,1280]{1,0:T(8,128)(2,1)}) %all-gather.3.cloned.1.call-update) | async-done | bytes 5242896 | tf_op jit(solution)/shard_map/weights/all_gather | solution.py:741
  176.4 42.5 %feed_forward.1 = bf16[96,2048]{1,0:T(8,128)(2,1)} custom-call(bf16[2,96,1024]{2,1,0:T(8,128)(2,1)} %get-tuple-element.7.rows_in_ref, f32[96,2048]{1,0:T(8,128)} %get-tuple-element.8.stream_ref, bf16[2048,1280]{1,0:T(8,128)(2,1)} %all-gather.3.cloned.1.call-done.gate_up_hbm, bf16[2048,640]{1,0:T(8,128)(2,1)} %all-gather.5.cloned.1.call-done.down_hbm), custom_call_target="tpu_custom_call" | custom-call | flops 20000000000 | bytes 8000000 | tf_op jit(solution)/shard_map/feed_forward/pallas_call | solution.py:312
  218.9 1.8 copy.23
Async XLA Ops:
  6.5 84.3 %all-gather.5.cloned.1.call-start = ((), (), s32[]{:S(2)}) async-start(), calls=%async_computation.1 | async-start | bytes 2703360 | tf_op jit(solution)/shard_map/weights/all_gather | solution.py:742
  7.3 169.2 %all-gather.3.cloned.1.call-start = ((), (), s32[]{:S(2)}) async-start(), calls=%async_computation | async-start | bytes 5406720 | tf_op jit(solution)/shard_map/weights/all_gather | solution.py:741
Sparse Core Ops, SparseCore 0:
  9.9 80.8 all-gather.4
  93.4 82.9 all-gather.2

commit v3 on v2

--- a/solution.py
+++ b/solution.py
@@ -35,6 +35,16 @@
 
 def dot_tn(a, b):
     return lax.dot_general(a, b, (((0,), (0,)), ((), ())), preferred_element_type=F32)
+
+
+def dot_tn_exact(a, b):
+    return lax.dot_general(
+        a,
+        b,
+        (((0,), (0,)), ((), ())),
+        precision=lax.Precision.HIGHEST,
+        preferred_element_type=F32,
+    )
 
 
 def two_parts(x):
@@ -159,186 +169,159 @@
         pl.semaphore_signal(barrier, inc=1, device_id={"tp": to}, device_id_type=MESH)
 
 
-def feed_forward_kernel(
-    rows_in_ref,
-    stream_ref,
-    gate_up_hbm,
-    down_hbm,
-    out_ref,
-    gate_up_ref,
-    down_ref,
-    rows_ref,
-    hidden_ref,
-    part_ref,
-    sib_ref,
-    pair_ref,
-    relay_ref,
-    arrived_ref,
-    sib_send,
-    sib_recv,
-    hop_send,
-    hop_recv,
-    load_sem,
-    row_send,
-    row_recv,
-    side_send,
-    side_recv,
-):
-    barrier = pltpu.get_barrier_semaphore()
-    greet_ring(barrier)
-    chip, core, right, left, sibling = ring_places()
-    load_gate_up = pltpu.make_async_copy(gate_up_hbm, gate_up_ref, load_sem.at[0])
-    load_down = pltpu.make_async_copy(down_hbm, down_ref, load_sem.at[1])
-    load_gate_up.start()
-    load_down.start()
-    here = pl.ds(pl.multiple_of(core * ROWS, ROWS), ROWS)
-    there = pl.ds(pl.multiple_of((1 - core) * ROWS, ROWS), ROWS)
-
-    def chip_at(d):
-        return lax.rem(chip + d, 4)
-
-    rows_ref[chip, :, here, :] = rows_in_ref[...]
-    pl.semaphore_wait(barrier, 3)
-
-    def hop(n):
-        d, h, to = (
-            (0, 0, right),
-            (0, 1, left),
-            (0, 1, right),
-            (0, 0, left),
-            (3, 0, right),
-            (1, 1, left),
-        )[n]
-        block = rows_ref.at[chip_at(d), h, here, :]
-        return remote(block, block, row_send.at[n], row_recv.at[n], to)
-
-    def arrival(n):
-        d, h = ((3, 0), (1, 1), (3, 1), (1, 0), (2, 0), (2, 1))[n]
-        block = rows_ref.at[chip_at(d), h, here, :]
-        return remote(block, block, row_send.at[n], row_recv.at[n], sibling)
-
-    def side(n):
-        d, h = ((0, 0), (0, 1), (1, 0), (1, 1), (3, 0), (3, 1), (2, 0), (2, 1))[n]
-        block = rows_ref.at[chip_at(d), h, here, :]
-        return remote(block, block, side_send.at[n], side_recv.at[n], sibling)
-
-    def side_arrival(n):
-        d, h = ((0, 0), (0, 1), (1, 0), (1, 1), (3, 0), (3, 1), (2, 0), (2, 1))[n]
-        block = rows_ref.at[chip_at(d), h, there, :]
-        return remote(block, block, side_send.at[n], side_recv.at[n], sibling)
-
-    for n in range(4):
-        hop(n).start()
-    side(0).start()
-    side(1).start()
-
-    ring = RingSum(
-        part_ref,
-        sib_ref,
-        pair_ref,
-        relay_ref,
-        arrived_ref,
-        (sib_send, sib_recv, hop_send, hop_recv),
-    )
-    ff_half = hidden_ref.shape[1]
-
-    def produce(d):
-        block = chip_at(d)
-        x = [rows_ref[block, 0], rows_ref[block, 1]]
-        for n in range(ff_half // 128):
-            cols = pl.ds(256 * n, 256)
-            both = dot_nn(x[0], gate_up_ref[0:HALF, cols]) + dot_nn(x[1], gate_up_ref[HALF:, cols])
-            gate_act, up_act = both[:, :128], both[:, 128:]
-            hidden_ref[:, pl.ds(128 * n, 128)] = (
-                gate_act * jax.nn.sigmoid(gate_act) * up_act
-            ).astype(BF16)
-        hidden = hidden_ref[...]
-        for h in range(2):
-            for n in range(HALF // 256):
-                part_ref[d, h, :, pl.ds(256 * n, 256)] = dot_nt(
-                    hidden, down_ref[pl.ds(h * HALF + 256 * n, 256), :]
-                ).astype(BF16)
-        ring.produced(d)
-
-    side_arrival(0).wait_recv()
-    side_arrival(1).wait_recv()
-    load_gate_up.wait()
-    load_down.wait()
-    produce(0)
-    arrival(0).wait_recv()
-    hop(4).start()
-    side(4).start()
-    arrival(1).wait_recv()
-    hop(5).start()
-    side(3).start()
-    arrival(2).wait_recv()
-    side(5).start()
-    arrival(3).wait_recv()
-    side(2).start()
-    side_arrival(4).wait_recv()
-    side_arrival(5).wait_recv()
-    produce(3)
-    side_arrival(2).wait_recv()
-    side_arrival(3).wait_recv()
-    arrival(4).wait_recv()
-    side(6).start()
-    arrival(5).wait_recv()
-    side(7).start()
-    ring.pass_on(3)
-    produce(1)
-    ring.pass_on(1)
-    side_arrival(6).wait_recv()
-    side_arrival(7).wait_recv()
-    produce(2)
-    ring.pass_on(2)
-    ring.pass_relayed()
-    ring.to_sibling(0).wait_recv()
-    ring.arrive()
-    for h in range(2):
-        out_ref[:, pl.ds(h * HALF, HALF)] = (
-            stream_ref[:, pl.ds(h * HALF, HALF)] + half_step * ring.result(h)
-        ).astype(BF16)
-    ring.drain()
-    for n in range(6):
-        hop(n).wait_send()
-    for n in range(8):
-        side(n).wait_send()
-
-
-def feed_forward(rows, stream, gate_up, down):
-    vmem = pl.BlockSpec(memory_space=pltpu.VMEM)
-    hbm = pl.BlockSpec(memory_space=pl.ANY)
-    ff = down.shape[1]
-    return pl.pallas_call(
-        feed_forward_kernel,
-        out_shape=jax.ShapeDtypeStruct((ROWS, 2 * HALF), BF16),
-        in_specs=[vmem, vmem, hbm, hbm],
-        out_specs=vmem,
-        scratch_shapes=[
-            pltpu.VMEM(gate_up.shape, BF16),
-            pltpu.VMEM(down.shape, BF16),
-            pltpu.VMEM((4, 2, 2 * ROWS, HALF), BF16),
-            pltpu.VMEM((2 * ROWS, ff), BF16),
-        ]
-        + RING_SUM_SCRATCH
-        + [
-            pltpu.SemaphoreType.DMA((2,)),
-            pltpu.SemaphoreType.DMA((6,)),
-            pltpu.SemaphoreType.DMA((6,)),
-            pltpu.SemaphoreType.DMA((8,)),
-            pltpu.SemaphoreType.DMA((8,)),
-        ],
-        compiler_params=pltpu.CompilerParams(
-            collective_id=1, has_side_effects=True, vmem_limit_bytes=56 * 1024 * 1024
-        ),
-        cost_estimate=pl.CostEstimate(
-            flops=20_000_000_000, bytes_accessed=8_000_000, transcendentals=0
-        ),
-        name="feed_forward",
-    )(rows, stream, gate_up, down)
-
-
-def mixing_kernel(
+class WeightGather:
+    def __init__(self, gate_up, down, n_z, n_y, send, recv):
+        self.gate_up, self.down, self.n_z, self.n_y = gate_up, down, n_z, n_y
+        self.send, self.recv = send, recv
+        self.z, self.y = lax.axis_index("sp_0"), lax.axis_index("sp_1")
+        self.block = gate_up.shape[0] // (n_z * n_y)
+        self.started = []
+
+    def z_at(self, d):
+        return lax.rem(self.z + d + self.n_z, self.n_z)
+
+    def y_at(self, d):
+        return lax.rem(self.y + d + self.n_y, self.n_y)
+
+    def rows(self, z, y, way=None):
+        start = (z * self.n_y + y) * self.block
+        if way is None:
+            return pl.ds(pl.multiple_of(start, 32), self.block)
+        half = self.block // 2
+        return pl.ds(pl.multiple_of(start + (0 if way > 0 else half), 32), half)
+
+    def group(self, z, way=None):
+        size = self.n_y * self.block
+        if way is None:
+            return pl.ds(pl.multiple_of(z * size, 32), size)
+        half = size // 2
+        return pl.ds(pl.multiple_of(z * size + (0 if way > 0 else half), 32), half)
+
+    def copy(self, ref, rows, n, device):
+        return pltpu.make_async_remote_copy(
+            src_ref=ref.at[rows],
+            dst_ref=ref.at[rows],
+            send_sem=self.send.at[n],
+            recv_sem=self.recv.at[n],
+            device_id=device,
+            device_id_type=MESH,
+        )
+
+    def zg(self, way, k, received=False):
+        n = (k - 1) * 2 + (way < 0)
+        half = way if k == self.n_z // 2 else None
+        to = {"sp_0": self.z_at(way)}
+        if received:
+            return self.copy(self.gate_up, self.rows(self.z_at(-way * k), self.y, half), n, to)
+        return self.copy(self.gate_up, self.rows(self.z_at(-way * (k - 1)), self.y, half), n, to)
+
+    def zd(self, way, k, received=False):
+        n = 8 + (k - 1) * 2 + (way < 0)
+        half = way if k == self.n_z // 2 else None
+        to = {"sp_0": self.z_at(way)}
+        if received:
+            return self.copy(self.down, self.group(self.z_at(-way * k), half), n, to)
+        return self.copy(self.down, self.group(self.z_at(-way * (k - 1)), half), n, to)
+
+    def yg(self, d, way, k, received=False):
+        n = 16 + (d + 3) * 4 + (k - 1) * 2 + (way < 0)
+        half = way if k == 2 else None
+        z = self.z_at(d)
+        to = {"sp_1": self.y_at(way)}
+        if received:
+            return self.copy(self.gate_up, self.rows(z, self.y_at(-way * k), half), n, to)
+        return self.copy(self.gate_up, self.rows(z, self.y_at(-way * (k - 1)), half), n, to)
+
+    def yd(self, way, k, received=False):
+        n = 48 + (k - 1) * 2 + (way < 0)
+        half = way if k == 2 else None
+        to = {"sp_1": self.y_at(way)}
+        if received:
+            return self.copy(self.down, self.rows(self.z, self.y_at(-way * k), half), n, to)
+        return self.copy(self.down, self.rows(self.z, self.y_at(-way * (k - 1)), half), n, to)
+
+    def start(self, maker, *args):
+        for way in (1, -1):
+            maker(*args[:-1], way, args[-1]).start()
+        self.started.append((maker, args))
+
+    def wait(self, maker, *args):
+        for way in (1, -1):
+            maker(*args[:-1], way, args[-1], received=True).wait_recv()
+
+    def step(self, n):
+        s, w = self.start, self.wait
+        if n == 0:
+            s(self.yd, 1)
+            s(self.zg, 1)
+            s(self.yg, 0, 1)
+        if n == 1:
+            w(self.yd, 1)
+            s(self.yd, 2)
+            w(self.zg, 1)
+            s(self.zg, 2)
+            s(self.yg, -1, 1)
+            s(self.yg, 1, 1)
+        if n == 2:
+            w(self.yd, 2)
+            s(self.zd, 1)
+            w(self.yg, 0, 1)
+            s(self.yg, 0, 2)
+        if n == 3:
+            w(self.zg, 2)
+            s(self.zg, 3)
+            s(self.yg, -2, 1)
+            s(self.yg, 2, 1)
+        if n == 4:
+            for d in (-1, 1):
+                w(self.yg, d, 1)
+                s(self.yg, d, 2)
+        if n == 5:
+            w(self.zd, 1)
+            s(self.zd, 2)
+        if n == 6:
+            w(self.zg, 3)
+            s(self.zg, 4)
+            s(self.yg, -3, 1)
+            s(self.yg, 3, 1)
+        if n == 7:
+            for d in (-2, 2):
+                w(self.yg, d, 1)
+                s(self.yg, d, 2)
+        if n == 8:
+            w(self.zd, 2)
+            s(self.zd, 3)
+        if n == 9:
+            w(self.zg, 4)
+            s(self.yg, 4, 1)
+        if n == 10:
+            for d in (-3, 3):
+                w(self.yg, d, 1)
+                s(self.yg, d, 2)
+        if n == 11:
+            w(self.zd, 3)
+            s(self.zd, 4)
+        if n == 12:
+            w(self.yg, 4, 1)
+            s(self.yg, 4, 2)
+
+    def gate_up_here(self):
+        for d in (0, -1, 1, -2, 2, -3, 3, 4):
+            self.wait(self.yg, d, 2)
+
+    def down_here(self):
+        self.wait(self.zd, 4)
+
+    def drain(self):
+        for maker, args in self.started:
+            for way in (1, -1):
+                maker(*args[:-1], way, args[-1]).wait_send()
+
+
+WEIGHT_COPIES = 52
+
+
+def layer_kernel(
     n_z,
     n_y,
     r_hbm,
@@ -354,7 +337,10 @@
     skip_ref,
     matrix_hbm,
     gain_ref,
-    rows_out_ref,
+    switch_hbm,
+    expand_hbm,
+    contract_hbm,
+    out_ref,
     stream_ref,
     r_ref,
     k_ref,
@@ -379,6 +365,17 @@
     recv_y_sem,
     send_z_sem,
     recv_z_sem,
+    gate_up_ref,
+    down_ref,
+    rows_ref,
+    hidden_ref,
+    weight_load_sem,
+    weight_send,
+    weight_recv,
+    row_send,
+    row_recv,
+    side_send,
+    side_recv,
     *ring_refs,
 ):
     length, width = r_ref.shape
@@ -400,7 +397,22 @@
             )
         )
     ]
-    for load in loads:
+    gather = WeightGather(gate_up_ref, down_ref, n_z, n_y, weight_send, weight_recv)
+    own_rows = gather.rows(place_z, place_y)
+    ff = down_ref.shape[1]
+    weight_loads = [
+        pltpu.make_async_copy(contract_hbm, down_ref.at[own_rows], weight_load_sem.at[0])
+    ]
+    for n in range(ff // 128):
+        for m, src in enumerate((switch_hbm, expand_hbm)):
+            weight_loads.append(
+                pltpu.make_async_copy(
+                    src.at[:, pl.ds(128 * n, 128)],
+                    gate_up_ref.at[own_rows, pl.ds(256 * n + 128 * m, 128)],
+                    weight_load_sem.at[1 + 2 * n + m],
+                )
+            )
+    for load in weight_loads + loads:
         load.start()
     barrier = pltpu.get_barrier_semaphore()
     greet_ring(barrier)
@@ -423,6 +435,12 @@
     j_idx = lane % C
     strict = j_idx < t_idx
     inclusive = j_idx <= t_idx
+    pick = jnp.where(
+        lax.broadcasted_iota(jnp.int32, (heads, width), 1) // C
+        == lax.broadcasted_iota(jnp.int32, (heads, width), 0),
+        1.0,
+        0.0,
+    ).astype(F32)
     eye = jnp.where(j_idx == t_idx, 1.0, 0.0).astype(F32)
     for n, b in enumerate(LEVELS):
         rb = (big_row % C) // b
@@ -454,16 +472,12 @@
     sm_ref[0:C, :] = jnp.zeros((C, width), F32)
     sm_ref[C:, :] = eye
 
-    def chunk(c, result):
+    def chunk(c, added, result):
         rows = pl.ds(pl.multiple_of(c * C, C), C)
         r = r_ref[rows, :].astype(F32)
         k = k_ref[rows, :].astype(F32)
         vb = v_ref[rows, :]
         v = vb.astype(F32)
-        afl = afl_ref[rows, :]
-        added = jnp.broadcast_to(afl[:, 0:1], (C, width))
-        for h in range(1, heads):
-            added = jnp.where(lane >= h * C, afl[:, h : h + 1], added)
         log_step = added - EXP_HALF * jax.nn.sigmoid(foff_ref[...] + fd_ref[rows, :].astype(F32))
         rate = jax.nn.sigmoid(soff_ref[...] + sd_ref[rows, :].astype(F32))
         k_hi, k_lo = two_parts(k * k)
@@ -524,8 +538,17 @@
         )
 
     def group(g, _):
+        for n in range(1, 6):
+
+            @pl.when(g == n)
+            def _():
+                gather.step(n)
+
+        added = dot_tn_exact(afl_ref[:, pl.ds(pl.multiple_of(g * C * TOGETHER, 128), C * TOGETHER)], pick)
         results = [[] for _ in range(TOGETHER)]
-        running = [chunk(g * TOGETHER + n, results[n]) for n in range(TOGETHER)]
+        running = [
+            chunk(g * TOGETHER + n, added[n * C : (n + 1) * C], results[n]) for n in range(TOGETHER)
+        ]
         while running:
             left_over = []
             for one in running:
@@ -546,6 +569,10 @@
         sm_ref[...] = sm
         return 0
 
+    for load in weight_loads:
+        load.wait()
+    pl.semaphore_wait(barrier, n_y - 1 + n_z - 1 + 3)
+    gather.step(0)
     for load in loads[:5]:
         load.wait()
     lax.fori_loop(0, length // (C * TOGETHER), group, 0)
@@ -557,7 +584,6 @@
     own = sm_ref[...].astype(BF16)
     packet_y[...] = own
     recv_y[place_y] = own
-    pl.semaphore_wait(barrier, n_y - 1 + n_z - 1 + 3)
 
     def copy_y(to, slot):
         return pltpu.make_async_remote_copy(
@@ -571,6 +597,7 @@
 
     for d in range(1, n_y):
         copy_y(lax.rem(place_y + d, n_y), place_y).start()
+    gather.step(6)
     for d in range(1, n_y):
         peer = lax.rem(place_y + n_y - d, n_y)
         copy_y(peer, peer).wait_recv()
@@ -597,6 +624,7 @@
         def _():
             copy_z(place_z + d, place_z).start()
 
+    gather.step(7)
     s_ref[...] = jnp.zeros((C, width), F32)
     for m in range(n_z - 1):
 
@@ -614,7 +642,7 @@
     loads[6].wait()
 
     span = 2 * ROWS
-    ring = RingSum(*ring_refs[:5], ring_refs[5:])
+    ring = RingSum(*ring_refs[:5], ring_refs[5:9])
 
     def produce(d):
         start = lax.rem(ring.chip + d, 4) * span
@@ -635,13 +663,17 @@
                 ).astype(BF16)
         ring.produced(d)
 
+    gather.step(8)
     produce(2)
     produce(1)
+    gather.step(9)
     ring.pass_on(2)
     produce(3)
     ring.pass_on(1)
+    gather.step(10)
     produce(0)
     ring.pass_on(3)
+    gather.step(11)
     ring.pass_relayed()
     ring.to_sibling(0).wait_recv()
     ring.arrive()
@@ -652,12 +684,119 @@
         stream_ref[:, cols] = stream
         squares = squares + jnp.sum(stream * stream, axis=1, keepdims=True)
     scale_rows = lax.rsqrt(squares * (1.0 / (2 * HALF)) + norm_eps)
+    chip, core, right, left, sibling = ring_places()
+    here = pl.ds(pl.multiple_of(core * ROWS, ROWS), ROWS)
+    there = pl.ds(pl.multiple_of((1 - core) * ROWS, ROWS), ROWS)
+
+    def chip_at(d):
+        return lax.rem(chip + d, 4)
+
     for h in range(2):
         cols = pl.ds(h * HALF, HALF)
-        rows_out_ref[h] = (stream_ref[:, cols] * scale_rows * gain_ref[:, cols]).astype(BF16)
+        rows_ref[chip, h, here, :] = (stream_ref[:, cols] * scale_rows * gain_ref[:, cols]).astype(
+            BF16
+        )
+
+    def hop(n):
+        d, h, to = (
+            (0, 0, right),
+            (0, 1, left),
+            (0, 1, right),
+            (0, 0, left),
+            (3, 0, right),
+            (1, 1, left),
+        )[n]
+        block = rows_ref.at[chip_at(d), h, here, :]
+        return remote(block, block, row_send.at[n], row_recv.at[n], to)
+
+    def arrival(n):
+        d, h = ((3, 0), (1, 1), (3, 1), (1, 0), (2, 0), (2, 1))[n]
+        block = rows_ref.at[chip_at(d), h, here, :]
+        return remote(block, block, row_send.at[n], row_recv.at[n], sibling)
+
+    def side(n):
+        d, h = ((0, 0), (0, 1), (1, 0), (1, 1), (3, 0), (3, 1), (2, 0), (2, 1))[n]
+        block = rows_ref.at[chip_at(d), h, here, :]
+        return remote(block, block, side_send.at[n], side_recv.at[n], sibling)
+
+    def side_arrival(n):
+        d, h = ((0, 0), (0, 1), (1, 0), (1, 1), (3, 0), (3, 1), (2, 0), (2, 1))[n]
+        block = rows_ref.at[chip_at(d), h, there, :]
+        return remote(block, block, side_send.at[n], side_recv.at[n], sibling)
+
+    for n in range(4):
+        hop(n).start()
+    side(0).start()
+    side(1).start()
+    gather.step(12)
+
+    ring_2 = RingSum(*ring_refs[9:14], ring_refs[14:])
+    ff_half = hidden_ref.shape[1]
+
+    def feed(d):
+        block = chip_at(d)
+        x = [rows_ref[block, 0], rows_ref[block, 1]]
+        for n in range(ff_half // 128):
+            cols = pl.ds(256 * n, 256)
+            both = dot_nn(x[0], gate_up_ref[0:HALF, cols]) + dot_nn(x[1], gate_up_ref[HALF:, cols])
+            gate_act, up_act = both[:, :128], both[:, 128:]
+            hidden_ref[:, pl.ds(128 * n, 128)] = (
+                gate_act * jax.nn.sigmoid(gate_act) * up_act
+            ).astype(BF16)
+        if d == 0:
+            gather.down_here()
+        hidden = hidden_ref[...]
+        for h in range(2):
+            for n in range(HALF // 256):
+                ring_2.part[d, h, :, pl.ds(256 * n, 256)] = dot_nt(
+                    hidden, down_ref[pl.ds(h * HALF + 256 * n, 256), :]
+                ).astype(BF16)
+        ring_2.produced(d)
+
+    side_arrival(0).wait_recv()
+    side_arrival(1).wait_recv()
+    gather.gate_up_here()
+    feed(0)
+    arrival(0).wait_recv()
+    hop(4).start()
+    side(4).start()
+    arrival(1).wait_recv()
+    hop(5).start()
+    side(3).start()
+    arrival(2).wait_recv()
+    side(5).start()
+    arrival(3).wait_recv()
+    side(2).start()
+    side_arrival(4).wait_recv()
+    side_arrival(5).wait_recv()
+    feed(3)
+    side_arrival(2).wait_recv()
+    side_arrival(3).wait_recv()
+    arrival(4).wait_recv()
+    side(6).start()
+    arrival(5).wait_recv()
+    side(7).start()
+    ring_2.pass_on(3)
+    feed(1)
+    ring_2.pass_on(1)
+    side_arrival(6).wait_recv()
+    side_arrival(7).wait_recv()
+    feed(2)
+    ring_2.pass_on(2)
+    ring_2.pass_relayed()
+    ring_2.to_sibling(0).wait_recv()
+    ring_2.arrive()
+    for h in range(2):
+        out_ref[:, pl.ds(h * HALF, HALF)] = (
+            stream_ref[:, pl.ds(h * HALF, HALF)] + half_step * ring_2.result(h)
+        ).astype(BF16)
+    ring_2.drain()
+    for n in range(6):
+        hop(n).wait_send()
+    for n in range(8):
+        side(n).wait_send()
     ring.drain()
-
-
+    gather.drain()
     for d in range(1, n_y):
         to = lax.rem(place_y + d, n_y)
         copy_y(to, to).wait_send()
@@ -668,23 +807,24 @@
             copy_z(place_z + d, place_z).wait_send()
 
 
-def mixed_rows_of(r, k, v, gate, fd, afl, foff, sd, soff, scale, skip, matrix, gain):
+def layer(r, k, v, gate, fd, afl, foff, sd, soff, scale, skip, matrix, gain, switch, expand, contract):
     n_z, n_y = lax.axis_size("sp_0"), lax.axis_size("sp_1")
     length, width = r.shape
+    ff = switch.shape[1]
+    depth = switch.shape[0] * n_z * n_y
     vmem = pl.BlockSpec(memory_space=pltpu.VMEM)
     hbm = pl.BlockSpec(memory_space=pl.ANY)
+    dma = pltpu.SemaphoreType.DMA
     return pl.pallas_call(
-        functools.partial(mixing_kernel, n_z, n_y),
-        out_shape=(
-            jax.ShapeDtypeStruct((2, ROWS, HALF), BF16),
-            jax.ShapeDtypeStruct((ROWS, 2 * HALF), F32),
-        ),
-        in_specs=[hbm] * 5 + [vmem, vmem, hbm, vmem, vmem, vmem, hbm, vmem],
-        out_specs=(vmem, vmem),
-        scratch_shapes=[pltpu.VMEM((length, width), BF16)] * 6
+        functools.partial(layer_kernel, n_z, n_y),
+        out_shape=jax.ShapeDtypeStruct((ROWS, 2 * HALF), BF16),
+        in_specs=[hbm] * 5 + [vmem, vmem, hbm, vmem, vmem, vmem, hbm, vmem, hbm, hbm, hbm],
+        out_specs=vmem,
+        scratch_shapes=[pltpu.VMEM((ROWS, 2 * HALF), F32)]
+        + [pltpu.VMEM((length, width), BF16)] * 6
         + [
             pltpu.VMEM((width, 2 * HALF), BF16),
-            pltpu.SemaphoreType.DMA((7,)),
+            dma((7,)),
             pltpu.VMEM((width, width), BF16),
             pltpu.VMEM((len(LEVELS), width, width), BF16),
             pltpu.VMEM((length, width), F32),
@@ -696,22 +836,34 @@
             pltpu.VMEM((2 * C, width), BF16),
             pltpu.VMEM((n_z, 2 * C, width), BF16),
             pltpu.VMEM((C, width), F32),
-            pltpu.SemaphoreType.DMA((n_y,)),
-            pltpu.SemaphoreType.DMA((n_y,)),
-            pltpu.SemaphoreType.DMA((n_z,)),
-            pltpu.SemaphoreType.DMA((n_z,)),
+            dma((n_y,)),
+            dma((n_y,)),
+            dma((n_z,)),
+            dma((n_z,)),
+            pltpu.VMEM((depth, 2 * ff), BF16),
+            pltpu.VMEM((depth, ff), BF16),
+            pltpu.VMEM((4, 2, 2 * ROWS, HALF), BF16),
+            pltpu.VMEM((2 * ROWS, ff), BF16),
+            dma((1 + 2 * (ff // 128),)),
+            dma((WEIGHT_COPIES,)),
+            dma((WEIGHT_COPIES,)),
+            dma((6,)),
+            dma((6,)),
+            dma((8,)),
+            dma((8,)),
         ]
+        + RING_SUM_SCRATCH
         + RING_SUM_SCRATCH,
         compiler_params=pltpu.CompilerParams(
-            collective_id=0, has_side_effects=True, vmem_limit_bytes=56 * 1024 * 1024
+            collective_id=0, has_side_effects=True, vmem_limit_bytes=60 * 1024 * 1024
         ),
         cost_estimate=pl.CostEstimate(
-            flops=40_000_000_000, bytes_accessed=3_000_000, transcendentals=0
+            flops=40_000_000_000, bytes_accessed=8_000_000, transcendentals=0
         ),
-        name="mixing",
+        name="layer",
     )(
-        r, k, v, gate, fd, afl, foff[None, :], sd, soff[None, :], scale[None, :], skip, matrix,
-        gain[None, :],
+        r, k, v, gate, fd, afl.T, foff[None, :], sd, soff[None, :], scale[None, :], skip, matrix,
+        gain[None, :], switch, expand, contract,
     )
 
 
@@ -733,14 +885,7 @@
     expand_matrix,
     contract_matrix,
 ):
-    depth, ff = switch_matrix.shape
-    paired = jnp.stack(
-        [switch_matrix.reshape(depth, -1, 128), expand_matrix.reshape(depth, -1, 128)], axis=2
-    ).reshape(depth, 2 * ff)
-    with jax.named_scope("weights"):
-        gate_up = lax.all_gather(paired, SP, axis=0, tiled=True)
-        down = lax.all_gather(contract_matrix, SP, axis=0, tiled=True)
-    rows, stream = mixed_rows_of(
+    return layer(
         acceptance_signal,
         lookup_mapped,
         payload_mapped,
@@ -754,8 +899,10 @@
         skip_stream,
         result_matrix,
         mlp_rescaler,
+        switch_matrix,
+        expand_matrix,
+        contract_matrix,
     )
-    return feed_forward(rows, stream, gate_up, down)
 
 
 def solution(mesh):

time: 228 us -> 113 us (0.50)
  the two profiles are of different devices: /device:TPU:1 before, /device:TPU:198 now
where the time goes in v3:
time: 113 us
  Pallas kernels  111 us (98%)
  local copies, waits for them, and re-layouts  1.77 us (2%)
    pallas_call x1, Pallas kernels, layer(): pl.pallas_call(functools.partial(layer_kernel, n_z, n_y), out_shape=jax.S...  111 us

profile of v3, /device:TPU:198, one launch (start us, length us, event | category | flops | bytes accessed | tf_op | source)
XLA Modules:
  0.0 112.8 jit_solution(18284975729773584279)
XLA Ops:
  0.0 111.0 %layer.1 = bf16[96,2048]{1,0:T(8,128)(2,1)} custom-call(bf16[768,256]{1,0:T(8,128)(2,1)} %r_hbm.1, bf16[768,256]{1,0:T(8,128)(2,1)} %k_hbm.1, bf16[768,256]{1,0:T(8,128)(2,1)} %v_hbm.1, bf16[768,256]{1,0:T(8,128)(2,1)} %gate_hbm.1, bf16[768,256]{1,0:T(8,128)(2,1)} %fd_hbm.1, f32[4,768]{1,0:T(4,128)} %bitcast.5, f32[1,256]{1,0:T(1,128)} %bitcast.7, ...), custom_call_target="tpu_custom_call" | custom-call | flops 40000000000 | bytes 8000000 | tf_op jit(solution)/shard_map/layer/pallas_call | solution.py:818
  111.0 1.8 %copy.18 = bf16[96,2048]{1,0:T(8,128)(2,1)} copy(bf16[96,2048]{1,0:T(8,128)(2,1)} %layer.1) | data formatting | bytes 786432

commit v4 on v3

--- a/solution.py
+++ b/solution.py
@@ -53,6 +53,8 @@
 
 
 ROWS = 96
+BATCHES = 2
+PIECE = ROWS // BATCHES
 HALF = 1024
 
 
@@ -81,8 +83,8 @@
         self.part, self.sib, self.pair, self.relay, self.arrived = part, sib, pair, relay, arrived
         self.sib_send, self.sib_recv, self.send, self.recv = sems
         self.chip, self.core, self.right, self.left, self.sibling = ring_places()
-        self.own = pl.ds(pl.multiple_of(self.core * ROWS, ROWS), ROWS)
-        self.other = pl.ds(pl.multiple_of((1 - self.core) * ROWS, ROWS), ROWS)
+        self.own = pl.ds(pl.multiple_of(self.core * PIECE, PIECE), PIECE)
+        self.other = pl.ds(pl.multiple_of((1 - self.core) * PIECE, PIECE), PIECE)
 
     def to_sibling(self, d):
         return remote(
@@ -151,11 +153,11 @@
 
 
 RING_SUM_SCRATCH = [
-    pltpu.VMEM((4, 2, 2 * ROWS, HALF), BF16),
-    pltpu.VMEM((4, 2, ROWS, HALF), BF16),
-    pltpu.VMEM((4, 2, ROWS, HALF), BF16),
-    pltpu.VMEM((2, ROWS, HALF), BF16),
-    pltpu.VMEM((2, 2, ROWS, HALF), BF16),
+    pltpu.VMEM((4, 2, 2 * PIECE, HALF), BF16),
+    pltpu.VMEM((4, 2, PIECE, HALF), BF16),
+    pltpu.VMEM((4, 2, PIECE, HALF), BF16),
+    pltpu.VMEM((2, PIECE, HALF), BF16),
+    pltpu.VMEM((2, 2, PIECE, HALF), BF16),
     pltpu.SemaphoreType.DMA((4,)),
     pltpu.SemaphoreType.DMA((4,)),
     pltpu.SemaphoreType.DMA((6,)),
@@ -249,59 +251,58 @@
         for way in (1, -1):
             maker(*args[:-1], way, args[-1], received=True).wait_recv()
 
+    def both(self, act, d, k):
+        for side in (-d, d):
+            act(self.yg, side, k)
+
     def step(self, n):
         s, w = self.start, self.wait
-        if n == 0:
+        if n == 1:
             s(self.yd, 1)
             s(self.zg, 1)
             s(self.yg, 0, 1)
-        if n == 1:
+        if n == 3:
             w(self.yd, 1)
             s(self.yd, 2)
             w(self.zg, 1)
             s(self.zg, 2)
-            s(self.yg, -1, 1)
-            s(self.yg, 1, 1)
-        if n == 2:
+            self.both(s, 1, 1)
+        if n == 4:
             w(self.yd, 2)
             s(self.zd, 1)
             w(self.yg, 0, 1)
             s(self.yg, 0, 2)
-        if n == 3:
+        if n == 5:
             w(self.zg, 2)
             s(self.zg, 3)
-            s(self.yg, -2, 1)
-            s(self.yg, 2, 1)
-        if n == 4:
-            for d in (-1, 1):
-                w(self.yg, d, 1)
-                s(self.yg, d, 2)
-        if n == 5:
+        if n == 6:
+            self.both(s, 2, 1)
+        if n == 7:
+            self.both(w, 1, 1)
+            self.both(s, 1, 2)
             w(self.zd, 1)
             s(self.zd, 2)
-        if n == 6:
+        if n == 8:
             w(self.zg, 3)
             s(self.zg, 4)
-            s(self.yg, -3, 1)
-            s(self.yg, 3, 1)
-        if n == 7:
-            for d in (-2, 2):
-                w(self.yg, d, 1)
-                s(self.yg, d, 2)
-        if n == 8:
+        if n == 15:
+            self.both(s, 3, 1)
+        if n == 9:
+            self.both(w, 2, 1)
+            self.both(s, 2, 2)
+        if n == 10:
             w(self.zd, 2)
             s(self.zd, 3)
-        if n == 9:
+        if n == 11:
             w(self.zg, 4)
             s(self.yg, 4, 1)
-        if n == 10:
-            for d in (-3, 3):
-                w(self.yg, d, 1)
-                s(self.yg, d, 2)
-        if n == 11:
+        if n == 14:
+            self.both(w, 3, 1)
+            self.both(s, 3, 2)
+        if n == 12:
             w(self.zd, 3)
             s(self.zd, 4)
-        if n == 12:
+        if n == 13:
             w(self.yg, 4, 1)
             s(self.yg, 4, 2)
 
@@ -360,7 +361,11 @@
     recv_y,
     packet_z,
     recv_z,
+    packet_in,
+    recv_in,
     s_ref,
+    send_in_sem,
+    recv_in_sem,
     send_y_sem,
     recv_y_sem,
     send_z_sem,
@@ -412,7 +417,7 @@
                     weight_load_sem.at[1 + 2 * n + m],
                 )
             )
-    for load in weight_loads + loads:
+    for load in loads[:5] + weight_loads + loads[5:]:
         load.start()
     barrier = pltpu.get_barrier_semaphore()
     greet_ring(barrier)
@@ -538,10 +543,14 @@
         )
 
     def group(g, _):
-        for n in range(1, 6):
+        for n in (1, 3, 4, 5):
 
             @pl.when(g == n)
             def _():
+                if n == 1:
+                    for load in weight_loads:
+                        load.wait()
+                    pl.semaphore_wait(barrier, n_y - 1 + n_z - 1 + 3)
                 gather.step(n)
 
         added = dot_tn_exact(afl_ref[:, pl.ds(pl.multiple_of(g * C * TOGETHER, 128), C * TOGETHER)], pick)
@@ -569,25 +578,33 @@
         sm_ref[...] = sm
         return 0
 
-    for load in weight_loads:
-        load.wait()
-    pl.semaphore_wait(barrier, n_y - 1 + n_z - 1 + 3)
-    gather.step(0)
     for load in loads[:5]:
         load.wait()
     lax.fori_loop(0, length // (C * TOGETHER), group, 0)
 
-    def followed_by(sm, packet):
-        prod = dot_nn(sm.astype(BF16), bd(packet[C:]))
-        return jnp.concatenate([prod[0:C] + packet[0:C].astype(F32), prod[C:]], axis=0)
-
-    own = sm_ref[...].astype(BF16)
-    packet_y[...] = own
-    recv_y[place_y] = own
+    low = lax.broadcasted_iota(jnp.int32, (C, 2 * C), 1) < C
+
+    def swapped(x):
+        return jnp.concatenate([x[:, C:], x[:, :C]], axis=1)
+
+    def map_of(packet):
+        wide = packet.astype(F32)
+        return jnp.concatenate(
+            [jnp.where(low, swapped(wide), 0.0), jnp.where(low, 0.0, wide)], axis=0
+        ).astype(BF16)
+
+    def followed_by(before, packet):
+        return dot_nn(before.astype(BF16), map_of(packet)) + jnp.where(low, packet.astype(F32), 0.0)
+
+    sm = sm_ref[...]
+    for h in range(heads):
+        cols = slice(h * C, (h + 1) * C)
+        packet_y[h] = jnp.concatenate([sm[0:C, cols], sm[C:, cols]], axis=1).astype(BF16)
+    recv_y[place_y] = packet_y[place_y]
 
     def copy_y(to, slot):
         return pltpu.make_async_remote_copy(
-            src_ref=packet_y,
+            src_ref=packet_y.at[to],
             dst_ref=recv_y.at[slot],
             send_sem=send_y_sem.at[to],
             recv_sem=recv_y_sem.at[slot],
@@ -601,12 +618,16 @@
     for d in range(1, n_y):
         peer = lax.rem(place_y + n_y - d, n_y)
         copy_y(peer, peer).wait_recv()
-    total = recv_y[0].astype(F32)
-    inside = jnp.concatenate([jnp.zeros((C, width), F32), eye], axis=0)
+    small_eye = jnp.where(
+        lax.broadcasted_iota(jnp.int32, (C, 2 * C), 1)
+        == lax.broadcasted_iota(jnp.int32, (C, 2 * C), 0) + C,
+        1.0,
+        0.0,
+    ).astype(F32)
+    insides = [small_eye, recv_y[0].astype(F32)]
     for m in range(1, n_y):
-        inside = jnp.where(place_y == m, total, inside)
-        total = followed_by(total, recv_y[m])
-    packet_z[...] = total.astype(BF16)
+        insides.append(followed_by(insides[m], recv_y[m]))
+    packet_z[...] = insides[n_y].astype(BF16)
 
     def copy_z(to, slot):
         return pltpu.make_async_remote_copy(
@@ -625,29 +646,70 @@
             copy_z(place_z + d, place_z).start()
 
     gather.step(7)
-    s_ref[...] = jnp.zeros((C, width), F32)
+    gather.step(8)
+    s_ref[...] = jnp.zeros((C, 2 * C), F32)
     for m in range(n_z - 1):
 
         @pl.when(m < place_z)
         def _():
             copy_z(m, m).wait_recv()
-            arrived = recv_z[m]
-            s_ref[...] = (
-                dot_nn(s_ref[...].astype(BF16), bd(arrived[C:])) + arrived[0:C].astype(F32)
-            )
-
-    incoming = dot_nn(s_ref[...].astype(BF16), bd(inside[C:])) + inside[0:C]
-    incoming_bd = bd(incoming)
+            s_ref[...] = jnp.where(low, followed_by(s_ref[...], recv_z[m]), 0.0)
+
+    before = s_ref[...].astype(BF16)
+    for m in range(n_y):
+        inside = insides[m]
+        packet_in[m] = (dot_nn(before, map_of(inside)) + jnp.where(low, inside, 0.0)).astype(BF16)
+    recv_in[place_y] = packet_in[place_y]
+
+    def copy_in(to, slot):
+        return pltpu.make_async_remote_copy(
+            src_ref=packet_in.at[to],
+            dst_ref=recv_in.at[slot],
+            send_sem=send_in_sem.at[to],
+            recv_sem=recv_in_sem.at[slot],
+            device_id={"sp_1": to},
+            device_id_type=MESH,
+        )
+
+    for d in range(1, n_y):
+        copy_in(lax.rem(place_y + d, n_y), place_y).start()
+    gather.step(15)
+    for d in range(1, n_y):
+        peer = lax.rem(place_y + n_y - d, n_y)
+        copy_in(peer, peer).wait_recv()
+    blocks = []
+    for h in range(heads):
+        state = recv_in[h].astype(F32)
+        state = jnp.where(low, state, 0.0) if h % 2 == 0 else jnp.where(low, 0.0, swapped(state))
+        empty = jnp.zeros((C, 2 * C), F32)
+        blocks.append(
+            jnp.concatenate([state if p == h // 2 else empty for p in range(heads // 2)], axis=1)
+        )
+    incoming_bd = jnp.concatenate(blocks, axis=0).astype(BF16)
     loads[5].wait()
     loads[6].wait()
 
-    span = 2 * ROWS
-    ring = RingSum(*ring_refs[:5], ring_refs[5:9])
-
-    def produce(d):
-        start = lax.rem(ring.chip + d, 4) * span
-        rows = pl.ds(pl.multiple_of(start, span), span)
-        outcome = local_ref[rows, :] + dot_nt(coef_ref[rows, :], incoming_bd)
+    span = 2 * PIECE
+    rings = [RingSum(*ring_refs[9 * n : 9 * n + 5], ring_refs[9 * n + 5 : 9 * n + 9]) for n in range(2 * BATCHES)]
+    chip, core, right, left, sibling = ring_places()
+    here = pl.ds(pl.multiple_of(core * PIECE, PIECE), PIECE)
+    there = pl.ds(pl.multiple_of((1 - core) * PIECE, PIECE), PIECE)
+
+    def chip_at(d):
+        return lax.rem(chip + d, 4)
+
+    def produce(b, d):
+        def taken(ref):
+            first = chip_at(d) * (2 * ROWS) + b * PIECE
+            return jnp.concatenate(
+                [
+                    ref[pl.ds(pl.multiple_of(first + n * ROWS, PIECE), PIECE), :].astype(F32)
+                    for n in range(2)
+                ],
+                axis=0,
+            )
+
+        outcome = taken(local_ref) + dot_nt(taken(coef_ref).astype(BF16), incoming_bd)
         o_hi, o_lo = two_parts(outcome)
         centre = dot_nn(jnp.concatenate([o_hi, o_lo], axis=0), mask_ref[...])
         away = outcome - (centre[0:span] + centre[span:]) * (1.0 / C)
@@ -655,49 +717,34 @@
         spread = dot_nn(jnp.concatenate([a_hi, a_lo], axis=0), mask_ref[...])
         spread = (spread[0:span] + spread[span:]) * (1.0 / C)
         normed = away * lax.rsqrt(spread + group_eps)
-        mixed = ((normed + extra_ref[rows, :]) * gate_ref[rows, :].astype(F32)).astype(BF16)
+        mixed = ((normed + taken(extra_ref)) * taken(gate_ref)).astype(BF16)
         for h in range(2):
             for n in range(HALF // 256):
-                ring.part[d, h, :, pl.ds(256 * n, 256)] = dot_nn(
+                rings[b].part[d, h, :, pl.ds(256 * n, 256)] = dot_nn(
                     mixed, matrix_ref[:, pl.ds(h * HALF + 256 * n, 256)]
                 ).astype(BF16)
-        ring.produced(d)
-
-    gather.step(8)
-    produce(2)
-    produce(1)
-    gather.step(9)
-    ring.pass_on(2)
-    produce(3)
-    ring.pass_on(1)
-    gather.step(10)
-    produce(0)
-    ring.pass_on(3)
-    gather.step(11)
-    ring.pass_relayed()
-    ring.to_sibling(0).wait_recv()
-    ring.arrive()
-    squares = jnp.zeros((ROWS, 1), F32)
-    for h in range(2):
-        cols = pl.ds(h * HALF, HALF)
-        stream = skip_ref[:, cols].astype(F32) + ring.result(h)
-        stream_ref[:, cols] = stream
-        squares = squares + jnp.sum(stream * stream, axis=1, keepdims=True)
-    scale_rows = lax.rsqrt(squares * (1.0 / (2 * HALF)) + norm_eps)
-    chip, core, right, left, sibling = ring_places()
-    here = pl.ds(pl.multiple_of(core * ROWS, ROWS), ROWS)
-    there = pl.ds(pl.multiple_of((1 - core) * ROWS, ROWS), ROWS)
-
-    def chip_at(d):
-        return lax.rem(chip + d, 4)
-
-    for h in range(2):
-        cols = pl.ds(h * HALF, HALF)
-        rows_ref[chip, h, here, :] = (stream_ref[:, cols] * scale_rows * gain_ref[:, cols]).astype(
-            BF16
-        )
-
-    def hop(n):
+        rings[b].produced(d)
+
+    def normed_rows(b):
+        rows = pl.ds(b * PIECE, PIECE)
+        squares = jnp.zeros((PIECE, 1), F32)
+        for h in range(2):
+            cols = pl.ds(h * HALF, HALF)
+            stream = skip_ref[rows, cols].astype(F32) + rings[b].result(h)
+            stream_ref[rows, cols] = stream
+            squares = squares + jnp.sum(stream * stream, axis=1, keepdims=True)
+        scale_rows = lax.rsqrt(squares * (1.0 / (2 * HALF)) + norm_eps)
+        for h in range(2):
+            cols = pl.ds(h * HALF, HALF)
+            rows_ref[b, chip, h, here, :] = (
+                stream_ref[rows, cols] * scale_rows * gain_ref[:, cols]
+            ).astype(BF16)
+        for n in range(4):
+            hop(b, n).start()
+        side(b, 0).start()
+        side(b, 1).start()
+
+    def hop(b, n):
         d, h, to = (
             (0, 0, right),
             (0, 1, left),
@@ -706,100 +753,146 @@
             (3, 0, right),
             (1, 1, left),
         )[n]
-        block = rows_ref.at[chip_at(d), h, here, :]
-        return remote(block, block, row_send.at[n], row_recv.at[n], to)
-
-    def arrival(n):
+        block = rows_ref.at[b, chip_at(d), h, here, :]
+        return remote(block, block, row_send.at[b, n], row_recv.at[b, n], to)
+
+    def arrival(b, n):
         d, h = ((3, 0), (1, 1), (3, 1), (1, 0), (2, 0), (2, 1))[n]
-        block = rows_ref.at[chip_at(d), h, here, :]
-        return remote(block, block, row_send.at[n], row_recv.at[n], sibling)
-
-    def side(n):
-        d, h = ((0, 0), (0, 1), (1, 0), (1, 1), (3, 0), (3, 1), (2, 0), (2, 1))[n]
-        block = rows_ref.at[chip_at(d), h, here, :]
-        return remote(block, block, side_send.at[n], side_recv.at[n], sibling)
-
-    def side_arrival(n):
-        d, h = ((0, 0), (0, 1), (1, 0), (1, 1), (3, 0), (3, 1), (2, 0), (2, 1))[n]
-        block = rows_ref.at[chip_at(d), h, there, :]
-        return remote(block, block, side_send.at[n], side_recv.at[n], sibling)
-
-    for n in range(4):
-        hop(n).start()
-    side(0).start()
-    side(1).start()
-    gather.step(12)
-
-    ring_2 = RingSum(*ring_refs[9:14], ring_refs[14:])
-    ff_half = hidden_ref.shape[1]
-
-    def feed(d):
-        block = chip_at(d)
-        x = [rows_ref[block, 0], rows_ref[block, 1]]
-        for n in range(ff_half // 128):
+        block = rows_ref.at[b, chip_at(d), h, here, :]
+        return remote(block, block, row_send.at[b, n], row_recv.at[b, n], sibling)
+
+    sides = ((0, 0), (0, 1), (1, 0), (1, 1), (3, 0), (3, 1), (2, 0), (2, 1))
+
+    def side(b, n):
+        d, h = sides[n]
+        block = rows_ref.at[b, chip_at(d), h, here, :]
+        return remote(block, block, side_send.at[b, n], side_recv.at[b, n], sibling)
+
+    def side_arrival(b, n):
+        d, h = sides[n]
+        block = rows_ref.at[b, chip_at(d), h, there, :]
+        return remote(block, block, side_send.at[b, n], side_recv.at[b, n], sibling)
+
+    def relay_rows(b):
+        arrival(b, 0).wait_recv()
+        hop(b, 4).start()
+        side(b, 4).start()
+        arrival(b, 1).wait_recv()
+        hop(b, 5).start()
+        side(b, 3).start()
+
+    def share_near(b):
+        arrival(b, 2).wait_recv()
+        side(b, 5).start()
+        arrival(b, 3).wait_recv()
+        side(b, 2).start()
+
+    def share_far(b):
+        arrival(b, 4).wait_recv()
+        side(b, 6).start()
+        arrival(b, 5).wait_recv()
+        side(b, 7).start()
+
+    def feed(*blocks):
+        for b, d in blocks:
+            for n in {0: (0, 1), 1: (2, 3), 3: (4, 5), 2: (6, 7)}[d]:
+                side_arrival(b, n).wait_recv()
+        x = [
+            jnp.concatenate([rows_ref[b, chip_at(d), h] for b, d in blocks], axis=0)
+            for h in range(2)
+        ]
+        filled = pl.ds(0, len(blocks) * span)
+        for n in range(hidden_ref.shape[1] // 128):
             cols = pl.ds(256 * n, 256)
             both = dot_nn(x[0], gate_up_ref[0:HALF, cols]) + dot_nn(x[1], gate_up_ref[HALF:, cols])
             gate_act, up_act = both[:, :128], both[:, 128:]
-            hidden_ref[:, pl.ds(128 * n, 128)] = (
+            hidden_ref[filled, pl.ds(128 * n, 128)] = (
                 gate_act * jax.nn.sigmoid(gate_act) * up_act
             ).astype(BF16)
-        if d == 0:
+        if blocks == ((0, 0),):
             gather.down_here()
-        hidden = hidden_ref[...]
+        hidden = hidden_ref[filled, :]
         for h in range(2):
             for n in range(HALF // 256):
-                ring_2.part[d, h, :, pl.ds(256 * n, 256)] = dot_nt(
-                    hidden, down_ref[pl.ds(h * HALF + 256 * n, 256), :]
-                ).astype(BF16)
-        ring_2.produced(d)
-
-    side_arrival(0).wait_recv()
-    side_arrival(1).wait_recv()
+                product = dot_nt(hidden, down_ref[pl.ds(h * HALF + 256 * n, 256), :]).astype(BF16)
+                for m, (b, d) in enumerate(blocks):
+                    rings[BATCHES + b].part[d, h, :, pl.ds(256 * n, 256)] = product[
+                        m * span : (m + 1) * span
+                    ]
+        for b, d in blocks:
+            rings[BATCHES + b].produced(d)
+
+    def finish(b):
+        ring = rings[BATCHES + b]
+        rows = pl.ds(b * PIECE, PIECE)
+        ring.to_sibling(0).wait_recv()
+        ring.arrive()
+        for h in range(2):
+            cols = pl.ds(h * HALF, HALF)
+            out_ref[rows, cols] = (stream_ref[rows, cols] + half_step * ring.result(h)).astype(BF16)
+
+    gather.step(9)
+    produce(0, 2)
+    gather.step(10)
+    produce(0, 1)
+    rings[0].pass_on(2)
+    produce(0, 3)
+    rings[0].pass_on(1)
+    produce(0, 0)
+    rings[0].pass_on(3)
+    produce(1, 2)
+    gather.step(11)
+    produce(1, 1)
+    rings[1].pass_on(2)
+    produce(1, 3)
+    gather.step(14)
+    rings[0].pass_relayed()
+    rings[1].pass_on(1)
+    produce(1, 0)
+    rings[1].pass_on(3)
+    gather.step(12)
+    rings[1].pass_relayed()
+    rings[0].to_sibling(0).wait_recv()
+    rings[0].arrive()
+    normed_rows(0)
+    gather.step(13)
+    rings[1].to_sibling(0).wait_recv()
+    rings[1].arrive()
+    normed_rows(1)
     gather.gate_up_here()
-    feed(0)
-    arrival(0).wait_recv()
-    hop(4).start()
-    side(4).start()
-    arrival(1).wait_recv()
-    hop(5).start()
-    side(3).start()
-    arrival(2).wait_recv()
-    side(5).start()
-    arrival(3).wait_recv()
-    side(2).start()
-    side_arrival(4).wait_recv()
-    side_arrival(5).wait_recv()
-    feed(3)
-    side_arrival(2).wait_recv()
-    side_arrival(3).wait_recv()
-    arrival(4).wait_recv()
-    side(6).start()
-    arrival(5).wait_recv()
-    side(7).start()
-    ring_2.pass_on(3)
-    feed(1)
-    ring_2.pass_on(1)
-    side_arrival(6).wait_recv()
-    side_arrival(7).wait_recv()
-    feed(2)
-    ring_2.pass_on(2)
-    ring_2.pass_relayed()
-    ring_2.to_sibling(0).wait_recv()
-    ring_2.arrive()
-    for h in range(2):
-        out_ref[:, pl.ds(h * HALF, HALF)] = (
-            stream_ref[:, pl.ds(h * HALF, HALF)] + half_step * ring_2.result(h)
-        ).astype(BF16)
-    ring_2.drain()
-    for n in range(6):
-        hop(n).wait_send()
-    for n in range(8):
-        side(n).wait_send()
-    ring.drain()
+    feed((0, 0))
+    relay_rows(0)
+    share_near(0)
+    feed((0, 3), (0, 1))
+    share_far(0)
+    relay_rows(1)
+    rings[2].pass_on(3)
+    rings[2].pass_on(1)
+    share_near(1)
+    feed((0, 2), (1, 0))
+    rings[2].pass_on(2)
+    share_far(1)
+    feed((1, 3), (1, 1))
+    rings[2].pass_relayed()
+    rings[3].pass_on(3)
+    rings[3].pass_on(1)
+    feed((1, 2))
+    rings[3].pass_on(2)
+    finish(0)
+    rings[3].pass_relayed()
+    finish(1)
+    for ring in rings:
+        ring.drain()
+    for b in range(BATCHES):
+        for n in range(6):
+            hop(b, n).wait_send()
+        for n in range(8):
+            side(b, n).wait_send()
     gather.drain()
     for d in range(1, n_y):
         to = lax.rem(place_y + d, n_y)
         copy_y(to, to).wait_send()
+        copy_in(to, to).wait_send()
     for d in range(1, n_z):
 
         @pl.when(place_z + d < n_z)
@@ -831,29 +924,32 @@
             pltpu.VMEM((length, width), BF16),
             pltpu.VMEM((length, width), F32),
             pltpu.VMEM((2 * C, width), F32),
-            pltpu.VMEM((2 * C, width), BF16),
-            pltpu.VMEM((n_y, 2 * C, width), BF16),
-            pltpu.VMEM((2 * C, width), BF16),
-            pltpu.VMEM((n_z, 2 * C, width), BF16),
-            pltpu.VMEM((C, width), F32),
+            pltpu.VMEM((n_y, C, 2 * C), BF16),
+            pltpu.VMEM((n_y, C, 2 * C), BF16),
+            pltpu.VMEM((C, 2 * C), BF16),
+            pltpu.VMEM((n_z, C, 2 * C), BF16),
+            pltpu.VMEM((n_y, C, 2 * C), BF16),
+            pltpu.VMEM((n_y, C, 2 * C), BF16),
+            pltpu.VMEM((C, 2 * C), F32),
+            dma((n_y,)),
+            dma((n_y,)),
             dma((n_y,)),
             dma((n_y,)),
             dma((n_z,)),
             dma((n_z,)),
             pltpu.VMEM((depth, 2 * ff), BF16),
             pltpu.VMEM((depth, ff), BF16),
-            pltpu.VMEM((4, 2, 2 * ROWS, HALF), BF16),
-            pltpu.VMEM((2 * ROWS, ff), BF16),
+            pltpu.VMEM((BATCHES, 4, 2, 2 * PIECE, HALF), BF16),
+            pltpu.VMEM((4 * PIECE, ff), BF16),
             dma((1 + 2 * (ff // 128),)),
             dma((WEIGHT_COPIES,)),
             dma((WEIGHT_COPIES,)),
-            dma((6,)),
-            dma((6,)),
-            dma((8,)),
-            dma((8,)),
+            dma((BATCHES, 6)),
+            dma((BATCHES, 6)),
+            dma((BATCHES, 8)),
+            dma((BATCHES, 8)),
         ]
-        + RING_SUM_SCRATCH
-        + RING_SUM_SCRATCH,
+        + RING_SUM_SCRATCH * (2 * BATCHES),
         compiler_params=pltpu.CompilerParams(
             collective_id=0, has_side_effects=True, vmem_limit_bytes=60 * 1024 * 1024
         ),

time: 113 us -> 97.2 us (0.86)
  the two profiles are of different devices: /device:TPU:198 before, /device:TPU:1 now
where the time goes in v4:
time: 97.2 us; the launch traced here: 96.6 us
  Pallas kernels  94.8 us (98%)
  local copies, waits for them, and re-layouts  1.77 us (2%)
    pallas_call x1, Pallas kernels, layer(): pl.pallas_call(functools.partial(layer_kernel, n_z, n_y), out_shape=jax.S...  94.8 us

profile of v4, /device:TPU:1, one launch (start us, length us, event | category | flops | bytes accessed | tf_op | source)
XLA Modules:
  0.0 96.6 jit_solution(1410001578316244056)
XLA Ops:
  0.0 94.8 %layer.1 = bf16[96,2048]{1,0:T(8,128)(2,1)} custom-call(bf16[768,256]{1,0:T(8,128)(2,1)} %r_hbm.1, bf16[768,256]{1,0:T(8,128)(2,1)} %k_hbm.1, bf16[768,256]{1,0:T(8,128)(2,1)} %v_hbm.1, bf16[768,256]{1,0:T(8,128)(2,1)} %gate_hbm.1, bf16[768,256]{1,0:T(8,128)(2,1)} %fd_hbm.1, f32[4,768]{1,0:T(4,128)} %bitcast.5, f32[1,256]{1,0:T(1,128)} %bitcast.7, ...), custom_call_target="tpu_custom_call" | custom-call | flops 40000000000 | bytes 8000000 | tf_op jit(solution)/shard_map/layer/pallas_call | solution.py:911
  94.8 1.8 %copy.18 = bf16[96,2048]{1,0:T(8,128)(2,1)} copy(bf16[96,2048]{1,0:T(8,128)(2,1)} %layer.1) | data formatting | bytes 786432

commit v5 on v4

--- a/solution.py
+++ b/solution.py
@@ -330,14 +330,14 @@
     v_hbm,
     gate_hbm,
     fd_hbm,
-    afl_ref,
-    foff_ref,
+    afl_hbm,
+    foff_hbm,
     sd_hbm,
-    soff_ref,
-    scale_ref,
-    skip_ref,
+    soff_hbm,
+    scale_hbm,
+    skip_hbm,
     matrix_hbm,
-    gain_ref,
+    gain_hbm,
     switch_hbm,
     expand_hbm,
     contract_hbm,
@@ -350,6 +350,12 @@
     fd_ref,
     sd_ref,
     matrix_ref,
+    afl_ref,
+    foff_ref,
+    soff_ref,
+    scale_ref,
+    skip_ref,
+    gain_ref,
     load_sem,
     mask_ref,
     level_ref,
@@ -363,7 +369,6 @@
     recv_z,
     packet_in,
     recv_in,
-    s_ref,
     send_in_sem,
     recv_in_sem,
     send_y_sem,
@@ -397,8 +402,14 @@
                 (v_hbm, v_ref),
                 (fd_hbm, fd_ref),
                 (sd_hbm, sd_ref),
+                (afl_hbm, afl_ref),
+                (foff_hbm, foff_ref),
+                (soff_hbm, soff_ref),
+                (scale_hbm, scale_ref),
                 (gate_hbm, gate_ref),
                 (matrix_hbm, matrix_ref),
+                (skip_hbm, skip_ref),
+                (gain_hbm, gain_ref),
             )
         )
     ]
@@ -417,7 +428,7 @@
                     weight_load_sem.at[1 + 2 * n + m],
                 )
             )
-    for load in loads[:5] + weight_loads + loads[5:]:
+    for load in loads[:9] + weight_loads + loads[9:]:
         load.start()
     barrier = pltpu.get_barrier_semaphore()
     greet_ring(barrier)
@@ -467,6 +478,20 @@
 
     def bd(x):
         return tiled(x) * mask_ref[...]
+
+    def bd2(x):
+        return jnp.concatenate([x.astype(BF16)] * 2, axis=0) * mask_ref[0 : 2 * C, 0 : 2 * C]
+
+    def paired(product, axis, a, x, y):
+        outs = []
+        for p in range(heads // 2):
+            cols = slice(p * 2 * C, (p + 1) * 2 * C)
+            right_side = jnp.concatenate([bd2(x[:, cols]), bd2(y[:, cols])], axis=axis)
+            outs.append(product(a[:, cols], right_side))
+        return (
+            jnp.concatenate([o[:, : 2 * C] for o in outs], axis=1),
+            jnp.concatenate([o[:, 2 * C :] for o in outs], axis=1),
+        )
 
     def diagonal_of(full):
         out = full[0:C]
@@ -506,8 +531,7 @@
         grow_rest = jnp.exp(end - mid)
         grow_end = jnp.exp(end)
         left = jnp.concatenate([before_unit, read_fwd], axis=0).astype(BF16)
-        by_key = dot_nt(left, bd(key_back))
-        by_erase = dot_nt(left, bd(erase_back))
+        by_key, by_erase = paired(dot_nt, 0, left, key_back, erase_back)
         yield
         key_both = jnp.concatenate(
             [jnp.where(strict, by_key[0:C], 0.0), jnp.where(inclusive, by_key[C:], 0.0)], axis=0
@@ -523,13 +547,15 @@
             inv = inv - dot_nn(half.astype(BF16), bd(inv))
             yield
         inv_b = inv.astype(BF16)
-        recalled = dot_nn(inv_b, bd(by_value[0:C]))
-        carried_map = dot_nn(inv_b, bd(before_unit * grow_mid))
+        recalled, carried_map = paired(
+            dot_nn, 1, inv_b, by_value[0:C], before_unit * grow_mid
+        )
         yield
         recalled_b = recalled.astype(BF16)
         carried_b = carried_map.astype(BF16)
-        local = by_value[C:] - dot_nn(erase_read, bd(recalled_b))
-        from_start = (read_fwd * grow_mid - dot_nn(erase_read, bd(carried_b))).astype(BF16)
+        local_less, start_less = paired(dot_nn, 1, erase_read, recalled_b, carried_b)
+        local = by_value[C:] - local_less
+        from_start = (read_fwd * grow_mid - start_less).astype(BF16)
         key_end = (key_back * grow_rest).astype(BF16)
         erase_end = (erase_back * grow_rest).astype(BF16)
         gain = dot_tn(
@@ -571,14 +597,15 @@
         for n in range(TOGETHER):
             rows, local, from_start, gain, loss, grow_end = results[n][0]
             sm_b = sm.astype(BF16)
-            local_ref[rows, :] = local + dot_nt(from_start, bd(sm_b[0:C]))
-            coef_ref[rows, :] = dot_nt(from_start, bd(sm_b[C:])).astype(BF16)
+            from_state, coef = paired(dot_nt, 0, from_start, sm_b[0:C], sm_b[C:])
+            local_ref[rows, :] = local + from_state
+            coef_ref[rows, :] = coef.astype(BF16)
             sm = sm * grow_end - dot_nn(sm_b, loss)
             sm = jnp.concatenate([sm[0:C] + gain, sm[C:]], axis=0)
         sm_ref[...] = sm
         return 0
 
-    for load in loads[:5]:
+    for load in loads[:9]:
         load.wait()
     lax.fori_loop(0, length // (C * TOGETHER), group, 0)
 
@@ -647,15 +674,23 @@
 
     gather.step(7)
     gather.step(8)
-    s_ref[...] = jnp.zeros((C, 2 * C), F32)
     for m in range(n_z - 1):
 
         @pl.when(m < place_z)
         def _():
             copy_z(m, m).wait_recv()
-            s_ref[...] = jnp.where(low, followed_by(s_ref[...], recv_z[m]), 0.0)
-
-    before = s_ref[...].astype(BF16)
+
+        @pl.when(m >= place_z)
+        def _():
+            recv_z[m] = small_eye.astype(BF16)
+
+    runs = [recv_z[m] for m in range(n_z - 1)]
+    while len(runs) > 1:
+        runs = [
+            followed_by(runs[m], runs[m + 1]) if m + 1 < len(runs) else runs[m]
+            for m in range(0, len(runs), 2)
+        ]
+    before = jnp.where(low, runs[0].astype(F32), 0.0).astype(BF16)
     for m in range(n_y):
         inside = insides[m]
         packet_in[m] = (dot_nn(before, map_of(inside)) + jnp.where(low, inside, 0.0)).astype(BF16)
@@ -686,8 +721,8 @@
             jnp.concatenate([state if p == h // 2 else empty for p in range(heads // 2)], axis=1)
         )
     incoming_bd = jnp.concatenate(blocks, axis=0).astype(BF16)
-    loads[5].wait()
-    loads[6].wait()
+    for load in loads[9:]:
+        load.wait()
 
     span = 2 * PIECE
     rings = [RingSum(*ring_refs[9 * n : 9 * n + 5], ring_refs[9 * n + 5 : 9 * n + 9]) for n in range(2 * BATCHES)]
@@ -833,9 +868,9 @@
 
     gather.step(9)
     produce(0, 2)
-    gather.step(10)
     produce(0, 1)
     rings[0].pass_on(2)
+    gather.step(10)
     produce(0, 3)
     rings[0].pass_on(1)
     produce(0, 0)
@@ -863,23 +898,24 @@
     feed((0, 0))
     relay_rows(0)
     share_near(0)
+    feed((1, 0))
+    relay_rows(1)
     feed((0, 3), (0, 1))
     share_far(0)
-    relay_rows(1)
+    share_near(1)
     rings[2].pass_on(3)
     rings[2].pass_on(1)
-    share_near(1)
-    feed((0, 2), (1, 0))
+    feed((0, 2))
+    share_far(1)
     rings[2].pass_on(2)
-    share_far(1)
+    feed((1, 2))
+    rings[2].pass_relayed()
+    rings[3].pass_on(2)
     feed((1, 3), (1, 1))
-    rings[2].pass_relayed()
     rings[3].pass_on(3)
     rings[3].pass_on(1)
-    feed((1, 2))
-    rings[3].pass_on(2)
+    rings[3].pass_relayed()
     finish(0)
-    rings[3].pass_relayed()
     finish(1)
     for ring in rings:
         ring.drain()
@@ -911,13 +947,19 @@
     return pl.pallas_call(
         functools.partial(layer_kernel, n_z, n_y),
         out_shape=jax.ShapeDtypeStruct((ROWS, 2 * HALF), BF16),
-        in_specs=[hbm] * 5 + [vmem, vmem, hbm, vmem, vmem, vmem, hbm, vmem, hbm, hbm, hbm],
+        in_specs=[hbm] * 16,
         out_specs=vmem,
         scratch_shapes=[pltpu.VMEM((ROWS, 2 * HALF), F32)]
         + [pltpu.VMEM((length, width), BF16)] * 6
         + [
             pltpu.VMEM((width, 2 * HALF), BF16),
-            dma((7,)),
+            pltpu.VMEM((width // C, length), F32),
+            pltpu.VMEM((1, width), F32),
+            pltpu.VMEM((1, width), F32),
+            pltpu.VMEM((1, width), F32),
+            pltpu.VMEM((ROWS, 2 * HALF), BF16),
+            pltpu.VMEM((1, 2 * HALF), F32),
+            dma((13,)),
             pltpu.VMEM((width, width), BF16),
             pltpu.VMEM((len(LEVELS), width, width), BF16),
             pltpu.VMEM((length, width), F32),
@@ -930,7 +972,6 @@
             pltpu.VMEM((n_z, C, 2 * C), BF16),
             pltpu.VMEM((n_y, C, 2 * C), BF16),
             pltpu.VMEM((n_y, C, 2 * C), BF16),
-            pltpu.VMEM((C, 2 * C), F32),
             dma((n_y,)),
             dma((n_y,)),
             dma((n_y,)),

time: 97.2 us -> 95.2 us (0.979)
  Pallas kernels: 94.8 us -> 93.3 us
    pallas_call x1, Pallas kernels: 94.8 us -> 93.3 us  [layer(): pl.pallas_call(functools.partial(layer_kernel, n_z, n_y), out_shape=jax.S...]
where the time goes in v5:
time: 95.2 us; the launch traced here: 95.1 us
  Pallas kernels  93.3 us (98%)
  local copies, waits for them, and re-layouts  1.77 us (2%)
    pallas_call x1, Pallas kernels, layer(): pl.pallas_call(functools.partial(layer_kernel, n_z, n_y), out_shape=jax.S...  93.3 us

profile of v5, /device:TPU:1, one launch (start us, length us, event | category | flops | bytes accessed | tf_op | source)
XLA Modules:
  0.0 95.1 jit_solution(7659105366808023666)
XLA Ops:
  0.0 93.3 %layer.1 = bf16[96,2048]{1,0:T(8,128)(2,1)} custom-call(bf16[768,256]{1,0:T(8,128)(2,1)} %r_hbm.1, bf16[768,256]{1,0:T(8,128)(2,1)} %k_hbm.1, bf16[768,256]{1,0:T(8,128)(2,1)} %v_hbm.1, bf16[768,256]{1,0:T(8,128)(2,1)} %gate_hbm.1, bf16[768,256]{1,0:T(8,128)(2,1)} %fd_hbm.1, f32[4,768]{1,0:T(4,128)} %bitcast.5, f32[1,256]{1,0:T(1,128)} %bitcast.7, ...), custom_call_target="tpu_custom_call" | custom-call | flops 40000000000 | bytes 8000000 | tf_op jit(solution)/shard_map/layer/pallas_call | solution.py:947
  93.3 1.8 %copy.18 = bf16[96,2048]{1,0:T(8,128)(2,1)} copy(bf16[96,2048]{1,0:T(8,128)(2,1)} %layer.1) | data formatting | bytes 786432

commit v6 on v5

--- a/solution.py
+++ b/solution.py
@@ -78,6 +78,10 @@
     )
 
 
+def all_sent(ref, sem):
+    pltpu.make_async_copy(ref, ref, sem).wait()
+
+
 class RingSum:
     def __init__(self, part, sib, pair, relay, arrived, sems):
         self.part, self.sib, self.pair, self.relay, self.arrived = part, sib, pair, relay, arrived
@@ -90,7 +94,7 @@
         return remote(
             self.part.at[d, :, self.other, :],
             self.sib.at[d],
-            self.sib_send.at[d],
+            self.sib_send.at[0],
             self.sib_recv.at[d],
             self.sibling,
         )
@@ -104,7 +108,7 @@
             (self.pair.at[1, 0], self.arrived.at[0, 0], self.right),
             (self.pair.at[3, 1], self.arrived.at[1, 1], self.left),
         )[n]
-        return remote(src, dst, self.send.at[n], self.recv.at[n], to)
+        return remote(src, dst, self.send.at[0], self.recv.at[n], to)
 
     def produced(self, d):
         self.to_sibling(d).start()
@@ -146,10 +150,8 @@
         )
 
     def drain(self):
-        for d in range(4):
-            self.to_sibling(d).wait_send()
-        for n in range(6):
-            self.hop(n).wait_send()
+        all_sent(self.sib, self.sib_send.at[0])
+        all_sent(self.pair.at[0:3], self.send.at[0])
 
 
 RING_SUM_SCRATCH = [
@@ -158,9 +160,9 @@
     pltpu.VMEM((4, 2, PIECE, HALF), BF16),
     pltpu.VMEM((2, PIECE, HALF), BF16),
     pltpu.VMEM((2, 2, PIECE, HALF), BF16),
+    pltpu.SemaphoreType.DMA((1,)),
     pltpu.SemaphoreType.DMA((4,)),
-    pltpu.SemaphoreType.DMA((4,)),
-    pltpu.SemaphoreType.DMA((6,)),
+    pltpu.SemaphoreType.DMA((1,)),
     pltpu.SemaphoreType.DMA((6,)),
 ]
 
@@ -177,7 +179,6 @@
         self.send, self.recv = send, recv
         self.z, self.y = lax.axis_index("sp_0"), lax.axis_index("sp_1")
         self.block = gate_up.shape[0] // (n_z * n_y)
-        self.started = []
 
     def z_at(self, d):
         return lax.rem(self.z + d + self.n_z, self.n_z)
@@ -203,7 +204,7 @@
         return pltpu.make_async_remote_copy(
             src_ref=ref.at[rows],
             dst_ref=ref.at[rows],
-            send_sem=self.send.at[n],
+            send_sem=self.send.at[0 if ref is self.gate_up else 1],
             recv_sem=self.recv.at[n],
             device_id=device,
             device_id_type=MESH,
@@ -245,7 +246,6 @@
     def start(self, maker, *args):
         for way in (1, -1):
             maker(*args[:-1], way, args[-1]).start()
-        self.started.append((maker, args))
 
     def wait(self, maker, *args):
         for way in (1, -1):
@@ -314,9 +314,9 @@
         self.wait(self.zd, 4)
 
     def drain(self):
-        for maker, args in self.started:
-            for way in (1, -1):
-                maker(*args[:-1], way, args[-1]).wait_send()
+        rows = self.gate_up.shape[0] - self.block
+        all_sent(self.gate_up.at[0:rows], self.send.at[0])
+        all_sent(self.down.at[0:rows], self.send.at[1])
 
 
 WEIGHT_COPIES = 52
@@ -425,7 +425,7 @@
                 pltpu.make_async_copy(
                     src.at[:, pl.ds(128 * n, 128)],
                     gate_up_ref.at[own_rows, pl.ds(256 * n + 128 * m, 128)],
-                    weight_load_sem.at[1 + 2 * n + m],
+                    weight_load_sem.at[1],
                 )
             )
     for load in loads[:9] + weight_loads + loads[9:]:
@@ -574,8 +574,8 @@
             @pl.when(g == n)
             def _():
                 if n == 1:
-                    for load in weight_loads:
-                        load.wait()
+                    weight_loads[0].wait()
+                    all_sent(gate_up_ref.at[own_rows], weight_load_sem.at[1])
                     pl.semaphore_wait(barrier, n_y - 1 + n_z - 1 + 3)
                 gather.step(n)
 
@@ -789,24 +789,24 @@
             (1, 1, left),
         )[n]
         block = rows_ref.at[b, chip_at(d), h, here, :]
-        return remote(block, block, row_send.at[b, n], row_recv.at[b, n], to)
+        return remote(block, block, row_send.at[b], row_recv.at[b, n], to)
 
     def arrival(b, n):
         d, h = ((3, 0), (1, 1), (3, 1), (1, 0), (2, 0), (2, 1))[n]
         block = rows_ref.at[b, chip_at(d), h, here, :]
-        return remote(block, block, row_send.at[b, n], row_recv.at[b, n], sibling)
+        return remote(block, block, row_send.at[b], row_recv.at[b, n], sibling)
 
     sides = ((0, 0), (0, 1), (1, 0), (1, 1), (3, 0), (3, 1), (2, 0), (2, 1))
 
     def side(b, n):
         d, h = sides[n]
         block = rows_ref.at[b, chip_at(d), h, here, :]
-        return remote(block, block, side_send.at[b, n], side_recv.at[b, n], sibling)
+        return remote(block, block, side_send.at[b], side_recv.at[b, n], sibling)
 
     def side_arrival(b, n):
         d, h = sides[n]
         block = rows_ref.at[b, chip_at(d), h, there, :]
-        return remote(block, block, side_send.at[b, n], side_recv.at[b, n], sibling)
+        return remote(block, block, side_send.at[b], side_recv.at[b, n], sibling)
 
     def relay_rows(b):
         arrival(b, 0).wait_recv()
@@ -885,11 +885,11 @@
     rings[1].pass_on(1)
     produce(1, 0)
     rings[1].pass_on(3)
-    gather.step(12)
     rings[1].pass_relayed()
     rings[0].to_sibling(0).wait_recv()
     rings[0].arrive()
     normed_rows(0)
+    gather.step(12)
     gather.step(13)
     rings[1].to_sibling(0).wait_recv()
     rings[1].arrive()
@@ -909,8 +909,8 @@
     share_far(1)
     rings[2].pass_on(2)
     feed((1, 2))
+    rings[3].pass_on(2)
     rings[2].pass_relayed()
-    rings[3].pass_on(2)
     feed((1, 3), (1, 1))
     rings[3].pass_on(3)
     rings[3].pass_on(1)
@@ -920,10 +920,8 @@
     for ring in rings:
         ring.drain()
     for b in range(BATCHES):
-        for n in range(6):
-            hop(b, n).wait_send()
-        for n in range(8):
-            side(b, n).wait_send()
+        all_sent(rows_ref.at[b, 0:3, :, 0:PIECE, :], row_send.at[b])
+        all_sent(rows_ref.at[b, :, :, 0:PIECE, :], side_send.at[b])
     gather.drain()
     for d in range(1, n_y):
         to = lax.rem(place_y + d, n_y)
@@ -982,12 +980,12 @@
             pltpu.VMEM((depth, ff), BF16),
             pltpu.VMEM((BATCHES, 4, 2, 2 * PIECE, HALF), BF16),
             pltpu.VMEM((4 * PIECE, ff), BF16),
-            dma((1 + 2 * (ff // 128),)),
+            dma((2,)),
+            dma((2,)),
             dma((WEIGHT_COPIES,)),
-            dma((WEIGHT_COPIES,)),
+            dma((BATCHES,)),
             dma((BATCHES, 6)),
-            dma((BATCHES, 6)),
-            dma((BATCHES, 8)),
+            dma((BATCHES,)),
             dma((BATCHES, 8)),
         ]
         + RING_SUM_SCRATCH * (2 * BATCHES),

time: 95.2 us -> 94 us (0.987)
  Pallas kernels: 93.3 us -> 92.2 us
    pallas_call x1, Pallas kernels: 93.3 us -> 92.2 us  [layer(): pl.pallas_call(functools.partial(layer_kernel, n_z, n_y), out_shape=jax.S...]
where the time goes in v6:
time: 94 us; the launch traced here: 93.9 us
  Pallas kernels  92.2 us (98%)
  local copies, waits for them, and re-layouts  1.77 us (2%)
    pallas_call x1, Pallas kernels, layer(): pl.pallas_call(functools.partial(layer_kernel, n_z, n_y), out_shape=jax.S...  92.2 us

profile of v6, /device:TPU:1, one launch (start us, length us, event | category | flops | bytes accessed | tf_op | source)
XLA Modules:
  0.0 93.9 jit_solution(2240290615113630058)
XLA Ops:
  0.0 92.2 %layer.1 = bf16[96,2048]{1,0:T(8,128)(2,1)} custom-call(bf16[768,256]{1,0:T(8,128)(2,1)} %r_hbm.1, bf16[768,256]{1,0:T(8,128)(2,1)} %k_hbm.1, bf16[768,256]{1,0:T(8,128)(2,1)} %v_hbm.1, bf16[768,256]{1,0:T(8,128)(2,1)} %gate_hbm.1, bf16[768,256]{1,0:T(8,128)(2,1)} %fd_hbm.1, f32[4,768]{1,0:T(4,128)} %bitcast.5, f32[1,256]{1,0:T(1,128)} %bitcast.7, ...), custom_call_target="tpu_custom_call" | custom-call | flops 40000000000 | bytes 8000000 | tf_op jit(solution)/shard_map/layer/pallas_call | solution.py:945
  92.2 1.8 %copy.18 = bf16[96,2048]{1,0:T(8,128)(2,1)} copy(bf16[96,2048]{1,0:T(8,128)(2,1)} %layer.1) | data formatting | bytes 786432

commit v7 on v6

--- a/solution.py
+++ b/solution.py
@@ -78,7 +78,7 @@
     )
 
 
-def all_sent(ref, sem):
+def all_moved(ref, sem):
     pltpu.make_async_copy(ref, ref, sem).wait()
 
 
@@ -108,7 +108,7 @@
             (self.pair.at[1, 0], self.arrived.at[0, 0], self.right),
             (self.pair.at[3, 1], self.arrived.at[1, 1], self.left),
         )[n]
-        return remote(src, dst, self.send.at[0], self.recv.at[n], to)
+        return remote(src, dst, self.send.at[0], self.recv.at[min(n, 2)], to)
 
     def produced(self, d):
         self.to_sibling(d).start()
@@ -139,8 +139,7 @@
         self.hop(5).start()
 
     def arrive(self):
-        for n in (2, 3, 4, 5):
-            self.hop(n).wait_recv()
+        all_moved(self.arrived, self.recv.at[2])
 
     def result(self, h):
         return (
@@ -150,8 +149,8 @@
         )
 
     def drain(self):
-        all_sent(self.sib, self.sib_send.at[0])
-        all_sent(self.pair.at[0:3], self.send.at[0])
+        all_moved(self.sib, self.sib_send.at[0])
+        all_moved(self.pair.at[0:3], self.send.at[0])
 
 
 RING_SUM_SCRATCH = [
@@ -163,7 +162,7 @@
     pltpu.SemaphoreType.DMA((1,)),
     pltpu.SemaphoreType.DMA((4,)),
     pltpu.SemaphoreType.DMA((1,)),
-    pltpu.SemaphoreType.DMA((6,)),
+    pltpu.SemaphoreType.DMA((3,)),
 ]
 
 
@@ -227,7 +226,7 @@
         return self.copy(self.down, self.group(self.z_at(-way * (k - 1)), half), n, to)
 
     def yg(self, d, way, k, received=False):
-        n = 16 + (d + 3) * 4 + (k - 1) * 2 + (way < 0)
+        n = 16 + (d + 3) * 2 + (way < 0) if k == 1 else 36
         half = way if k == 2 else None
         z = self.z_at(d)
         to = {"sp_1": self.y_at(way)}
@@ -236,7 +235,7 @@
         return self.copy(self.gate_up, self.rows(z, self.y_at(-way * (k - 1)), half), n, to)
 
     def yd(self, way, k, received=False):
-        n = 48 + (k - 1) * 2 + (way < 0)
+        n = 32 + (k - 1) * 2 + (way < 0)
         half = way if k == 2 else None
         to = {"sp_1": self.y_at(way)}
         if received:
@@ -307,19 +306,18 @@
             s(self.yg, 4, 2)
 
     def gate_up_here(self):
-        for d in (0, -1, 1, -2, 2, -3, 3, 4):
-            self.wait(self.yg, d, 2)
+        all_moved(self.gate_up.at[0 : self.n_z * self.block], self.recv.at[36])
 
     def down_here(self):
         self.wait(self.zd, 4)
 
     def drain(self):
         rows = self.gate_up.shape[0] - self.block
-        all_sent(self.gate_up.at[0:rows], self.send.at[0])
-        all_sent(self.down.at[0:rows], self.send.at[1])
-
-
-WEIGHT_COPIES = 52
+        all_moved(self.gate_up.at[0:rows], self.send.at[0])
+        all_moved(self.down.at[0:rows], self.send.at[1])
+
+
+WEIGHT_ARRIVALS = 37
 
 
 def layer_kernel(
@@ -575,7 +573,7 @@
             def _():
                 if n == 1:
                     weight_loads[0].wait()
-                    all_sent(gate_up_ref.at[own_rows], weight_load_sem.at[1])
+                    all_moved(gate_up_ref.at[own_rows], weight_load_sem.at[1])
                     pl.semaphore_wait(barrier, n_y - 1 + n_z - 1 + 3)
                 gather.step(n)
 
@@ -801,12 +799,7 @@
     def side(b, n):
         d, h = sides[n]
         block = rows_ref.at[b, chip_at(d), h, here, :]
-        return remote(block, block, side_send.at[b], side_recv.at[b, n], sibling)
-
-    def side_arrival(b, n):
-        d, h = sides[n]
-        block = rows_ref.at[b, chip_at(d), h, there, :]
-        return remote(block, block, side_send.at[b], side_recv.at[b, n], sibling)
+        return remote(block, block, side_send.at[b], side_recv.at[b, n // 2], sibling)
 
     def relay_rows(b):
         arrival(b, 0).wait_recv()
@@ -830,8 +823,7 @@
 
     def feed(*blocks):
         for b, d in blocks:
-            for n in {0: (0, 1), 1: (2, 3), 3: (4, 5), 2: (6, 7)}[d]:
-                side_arrival(b, n).wait_recv()
+            all_moved(rows_ref.at[b, chip_at(d), :, there, :], side_recv.at[b, (0, 1, 3, 2)[d]])
         x = [
             jnp.concatenate([rows_ref[b, chip_at(d), h] for b, d in blocks], axis=0)
             for h in range(2)
@@ -869,9 +861,9 @@
     gather.step(9)
     produce(0, 2)
     produce(0, 1)
+    produce(0, 3)
     rings[0].pass_on(2)
     gather.step(10)
-    produce(0, 3)
     rings[0].pass_on(1)
     produce(0, 0)
     rings[0].pass_on(3)
@@ -920,8 +912,8 @@
     for ring in rings:
         ring.drain()
     for b in range(BATCHES):
-        all_sent(rows_ref.at[b, 0:3, :, 0:PIECE, :], row_send.at[b])
-        all_sent(rows_ref.at[b, :, :, 0:PIECE, :], side_send.at[b])
+        all_moved(rows_ref.at[b, 0:3, :, 0:PIECE, :], row_send.at[b])
+        all_moved(rows_ref.at[b, :, :, 0:PIECE, :], side_send.at[b])
     gather.drain()
     for d in range(1, n_y):
         to = lax.rem(place_y + d, n_y)
@@ -982,11 +974,11 @@
             pltpu.VMEM((4 * PIECE, ff), BF16),
             dma((2,)),
             dma((2,)),
-            dma((WEIGHT_COPIES,)),
+            dma((WEIGHT_ARRIVALS,)),
             dma((BATCHES,)),
             dma((BATCHES, 6)),
             dma((BATCHES,)),
-            dma((BATCHES, 8)),
+            dma((BATCHES, 4)),
         ]
         + RING_SUM_SCRATCH * (2 * BATCHES),
         compiler_params=pltpu.CompilerParams(

time: 94 us -> 93.2 us (level)
  no operation moved by 1% of the time
where the time goes in v7:
time: 93.2 us; the launch traced here: 93.1 us
  Pallas kernels  91.3 us (98%)
  local copies, waits for them, and re-layouts  1.77 us (2%)
    pallas_call x1, Pallas kernels, layer(): pl.pallas_call(functools.partial(layer_kernel, n_z, n_y), out_shape=jax.S...  91.3 us

profile of v7, /device:TPU:1, one launch (start us, length us, event | category | flops | bytes accessed | tf_op | source)
XLA Modules:
  0.0 93.1 jit_solution(3529093411467249516)
XLA Ops:
  0.0 91.3 %layer.1 = bf16[96,2048]{1,0:T(8,128)(2,1)} custom-call(bf16[768,256]{1,0:T(8,128)(2,1)} %r_hbm.1, bf16[768,256]{1,0:T(8,128)(2,1)} %k_hbm.1, bf16[768,256]{1,0:T(8,128)(2,1)} %v_hbm.1, bf16[768,256]{1,0:T(8,128)(2,1)} %gate_hbm.1, bf16[768,256]{1,0:T(8,128)(2,1)} %fd_hbm.1, f32[4,768]{1,0:T(4,128)} %bitcast.5, f32[1,256]{1,0:T(1,128)} %bitcast.7, ...), custom_call_target="tpu_custom_call" | custom-call | flops 40000000000 | bytes 8000000 | tf_op jit(solution)/shard_map/layer/pallas_call | solution.py:937
  91.3 1.8 %copy.18 = bf16[96,2048]{1,0:T(8,128)(2,1)} copy(bf16[96,2048]{1,0:T(8,128)(2,1)} %layer.1) | data formatting | bytes 786432
